TPU v7x, 256 devices: a whole 4x4x8 slice. The times are simulated.
256 devices in a mesh: kv: 32 (over z, x), tp: 8 (over y, core).
Axes of the slice: x: 4, y: 4, z: 8, core: 2. Of those that a mesh axis runs over, the one named last changes fastest.
Arguments:
- tokens: bfloat16 [4096, 2048], P('kv', 'tp'), may hold values from -6 to 6
- states: float32 [4096, 16, 64, 64], P('kv', 'tp'), may hold values from -6 to 6
- mix_gain: bfloat16 [2048], replicated, may hold values from 0.099609375 to 1.8984375
- w_query: bfloat16 [2048, 1024], P(None, 'tp'), may hold values from -0.125 to 0.125
- w_key: bfloat16 [2048, 1024], P(None, 'tp'), may hold values from -0.125 to 0.125
- w_value: bfloat16 [2048, 1024], P(None, 'tp'), may hold values from -0.125 to 0.125
- w_gate: bfloat16 [2048, 1024], P(None, 'tp'), may hold values from -0.125 to 0.125
- head_gain: bfloat16 [1024], P('tp'), may hold values from 0.099609375 to 1.8984375
- w_output: bfloat16 [1024, 2048], P('tp'), may hold values from -0.1875 to 0.1875
- channel_gain: bfloat16 [2048], replicated, may hold values from 0.099609375 to 1.8984375
- w_up: bfloat16 [2048, 8192], P(None, 'kv'), may hold values from -0.125 to 0.125
- w_down: bfloat16 [8192, 2048], P('kv'), may hold values from -0.0625 to 0.0625
Outputs:
- layer_out: bfloat16 [4096, 2048], P('kv', 'tp')
- new_states: float32 [4096, 16, 64, 64], P('kv', 'tp')
All inputs are finite; a program needn't handle non-finite values.
Results may differ from a plain program's by a relative error of at most 0.019.
Values may be sent and summed in bfloat16 or wider, within the bound.
A program may use at most 64 MiB of HBM per device.

v0:
```python
import jax
import jax.numpy as jnp
from jax import lax
from jax.sharding import Mesh
from jax.sharding import PartitionSpec as P

HEADS = 16
POS = 16384
KV = ("kv_0", "kv_1")


EPSILON = 1e-06
ROTARY_BASE = 10000.0


def in_order(tiles, dim):
    tiles = jnp.moveaxis(tiles, 0, dim)
    dims = tiles.shape
    return tiles.reshape(*dims[:dim], dims[dim] * dims[dim + 1], *dims[dim + 2 :])


def copy_for_each(array, axis):
    count = lax.axis_size(axis)
    return lax.all_to_all(
        jnp.broadcast_to(array[None], (count, *array.shape)), axis, 0, 0, tiled=True
    )


def gathered_copies(array, axis, dim):
    return in_order(copy_for_each(array, axis), dim)


def in_blocks(array, dim, count):
    dims = array.shape
    tiles = array.reshape(*dims[:dim], count, dims[dim] // count, *dims[dim + 1 :])
    return jnp.moveaxis(tiles, dim, 0)


def summed_on_arrival(array, axis, dim):
    count = lax.axis_size(axis)
    tiles = lax.all_to_all(in_blocks(array, dim, count), axis, 0, 0, tiled=True)
    return jnp.sum(tiles.astype(jnp.float32), axis=0)


def gathered_by_axis(array, axes, dim):
    if not axes:
        return array
    nearer = lax.all_gather(array, axes[-1], axis=dim, tiled=True)
    return gathered_by_axis(nearer, axes[:-1], dim)


def rotate(vectors):
    half_size = vectors.shape[-1] // 2
    frequency = ROTARY_BASE ** (-jnp.arange(half_size, dtype=jnp.float32) / half_size)
    angles = POS * frequency
    cosine = jnp.cos(angles)
    sines = jnp.sin(angles)
    first_half = vectors[..., :half_size]
    second = vectors[..., half_size:]
    return jnp.concatenate(
        [first_half * cosine - second * sines, first_half * sines + second * cosine], axis=-1
    )


def retain(normed, states, w_query, w_key, w_value, w_gate, head_gain, head_ids):
    row_count = states.shape[0]
    head_count = states.shape[1]
    head_size = states.shape[2]

    def project(weight):
        return jnp.dot(normed, weight, preferred_element_type=jnp.float32).reshape(
            row_count, head_count, head_size
        )

    queries = rotate(project(w_query)) * head_size ** (-0.5)
    keys_now = rotate(project(w_key))
    values = project(w_value)
    gating = jnp.dot(normed, w_gate, preferred_element_type=jnp.float32)
    decays = 1.0 - jnp.exp2(-1.0 - 11.0 * head_ids / (HEADS - 1))
    new_states = (
        decays[None, :, None, None] * states + keys_now[:, :, :, None] * values[:, :, None, :]
    )
    output = jnp.einsum("bhk,bhkv->bhv", queries, new_states, precision=lax.Precision.HIGHEST)
    center = output - jnp.mean(output, axis=-1, keepdims=True)
    spread = jnp.mean(center * center, axis=-1, keepdims=True)
    scaled = (
        center
        * lax.rsqrt(spread + EPSILON)
        * head_gain.astype(jnp.float32).reshape(head_count, head_size)
    )
    gated_out = (scaled.reshape(row_count, head_count * head_size) * jax.nn.silu(gating)).astype(
        jnp.bfloat16
    )
    return (gated_out, new_states)


def activate(everyone, channel_gain, w_up):
    spread_rows = everyone.astype(jnp.float32)
    second_rms = lax.rsqrt(jnp.mean(spread_rows * spread_rows, axis=1, keepdims=True) + EPSILON)
    scaled = (spread_rows * channel_gain.astype(jnp.float32)).astype(jnp.bfloat16)
    hidden = jnp.dot(scaled, w_up, preferred_element_type=jnp.float32) * second_rms
    return jnp.square(jax.nn.relu(hidden)).astype(jnp.bfloat16)


def local(
    tokens,
    states,
    mix_gain,
    w_query,
    w_key,
    w_value,
    w_gate,
    head_gain,
    w_output,
    channel_gain,
    w_up,
    w_down,
):
    full_rows = gathered_copies(tokens, "tp", 1)
    widened = full_rows.astype(jnp.float32)
    inverse_rms = lax.rsqrt(jnp.mean(widened * widened, axis=1, keepdims=True) + EPSILON)
    normed = (widened * inverse_rms * mix_gain.astype(jnp.float32)).astype(jnp.bfloat16)
    local_heads = states.shape[1]
    tp_index = lax.axis_index("tp")
    head_ids = (tp_index * local_heads + jnp.arange(local_heads)).astype(jnp.float32)
    gated_out, new_states = retain(
        normed, states, w_query, w_key, w_value, w_gate, head_gain, head_ids
    )
    partial_value = jnp.dot(gated_out, w_output, preferred_element_type=jnp.float32)
    attended = summed_on_arrival(partial_value.astype(jnp.bfloat16), "tp", 0)
    share_rows = attended.shape[0]
    own_rows = lax.dynamic_slice_in_dim(full_rows, tp_index * share_rows, share_rows, 0)
    middle = (own_rows.astype(jnp.float32) + attended).astype(jnp.bfloat16)
    everyone = gathered_by_axis(middle, KV, 0)
    activated = activate(everyone, channel_gain, w_up)
    down_sum = summed_on_arrival(
        jnp.dot(activated, w_down, preferred_element_type=jnp.float32).astype(jnp.bfloat16), KV, 0
    )
    finished = (middle.astype(jnp.float32) + down_sum).astype(jnp.bfloat16)
    layer_out = lax.all_to_all(finished, "tp", split_axis=1, concat_axis=0, tiled=True)
    return (layer_out, new_states)


def solution(mesh):
    torus = Mesh(mesh.devices.reshape(8, 4, mesh.shape["tp"]), ("kv_0", "kv_1", "tp"))
    in_specs = (
        P(KV, "tp"),
        P(KV, "tp", None, None),
        P(),
        P(None, "tp"),
        P(None, "tp"),
        P(None, "tp"),
        P(None, "tp"),
        P("tp"),
        P("tp", None),
        P(),
        P(None, KV),
        P(KV, None),
    )
    out_specs = (P(KV, "tp"), P(KV, "tp", None, None))
    return jax.shard_map(local, mesh=torus, in_specs=in_specs, out_specs=out_specs, check_vma=False)
```

profile of v0, /device:TPU:1, one launch (start us, length us, event | category | flops | bytes accessed | tf_op | source)
XLA Modules:
  0.0 178.3 jit_solution(15148791007178584661)
XLA Ops:
  7.2 1.8 broadcast_in_dim.2
  8.9 6.6 %all-to-all-start = ((bf16[8,128,256]{2,1,0:T(8,128)(2,1)}), bf16[8,128,256]{2,1,0:T(8,128)(2,1)S(1)}, u32[]{:S(2)}, u32[]{:S(2)}) async-start(bf16[8,128,256]{2,1,0:T(8,128)(2,1)} %broadcast_in_dim.2), calls=%async_computation | async-start | bytes 1048576 | tf_op jit(solution)/shard_map/all_to_all | solution.py:24
  15.5 0.7 mul.214
  16.2 0.7 convert_element_type.71
  16.9 0.7 reshape.120
  17.6 2.0 %copy.43 = bf16[2048,128]{0,1:T(8,128)(2,1)} copy(bf16[2048,128]{1,0:T(8,128)(2,1)} %param.15) | data formatting | bytes 1048576 | tf_op args[3]
  19.7 1.2 copy.45
  20.9 1.2 copy.47
  22.3 2.6 %all-to-all-done = bf16[8,128,256]{2,1,0:T(8,128)(2,1)S(1)} async-done(((bf16[8,128,256]{2,1,0:T(8,128)(2,1)}), bf16[8,128,256]{2,1,0:T(8,128)(2,1)S(1)}, u32[]{:S(2)}, u32[]{:S(2)}) %all-to-all-start) | async-done | bytes 524320 | tf_op jit(solution)/shard_map/all_to_all | solution.py:24
  25.5 0.3 fusion.21
  25.8 1.7 fusion.32
  27.5 0.3 fusion.33
  28.2 3.1 %multiply_reduce_fusion = (f32[128,2,64]{0,2,1:T(8,128)S(1)}, f32[128,2,64,64]{0,3,2,1:T(8,128)}) fusion(f32[128,2,64]{0,2,1:T(8,128)S(1)} %get-tuple-element.10, f32[128,2,64]{0,2,1:T(8,128)S(1)} %fusion.34, f32[128,2,64]{0,2,1:T(8,128)S(1)} %get-tuple-element.11, f32[128,2,64,64]{0,3,2,1:T(8,128)S(1)} %copy-done.1, f32[2]{0:T(128)S(1)} %exponential_subtract_fusion), kind=kLoop, calls=%fused_computation.4 | loop fusion | flops 5226496 | bytes 8650760 | tf_op jit(solution)/shard_map/bhk,bhkv->bhv/dot_general | solution.py:83
  31.7 1.7 convolution_convert_fusion.1
  33.4 4.3 %all-to-all-start.1 = ((bf16[8,16,2048]{2,1,0:T(8,128)(2,1)}), bf16[8,16,2048]{2,1,0:T(8,128)(2,1)S(1)}, u32[]{:S(2)}, u32[]{:S(2)}) async-start(bf16[8,16,2048]{2,1,0:T(8,128)(2,1)} %bitcast.14), calls=%async_computation.1 | async-start | bytes 1048576 | tf_op jit(solution)/shard_map/all_to_all | solution.py:41
  38.1 9.0 %all-to-all-done.1 = bf16[8,16,2048]{2,1,0:T(8,128)(2,1)S(1)} async-done(((bf16[8,16,2048]{2,1,0:T(8,128)(2,1)}), bf16[8,16,2048]{2,1,0:T(8,128)(2,1)S(1)}, u32[]{:S(2)}, u32[]{:S(2)}) %all-to-all-start.1) | async-done | bytes 524320 | tf_op jit(solution)/shard_map/all_to_all | solution.py:41
  47.2 10.7 %all_gather.6 = bf16[64,2048]{1,0:T(8,128)(2,1)} all-gather(bf16[16,2048]{1,0:T(8,128)(2,1)S(1)} %add_convert_fusion.1), channel_id=1, replica_groups=mesh['kv_0'=8,'kv_1'=4,'tp'=8] {'kv_1'}, dimensions={0}, use_global_device_ids=true | all-gather | bytes 327680 | tf_op jit(solution)/shard_map/all_gather | solution.py:48
  57.9 39.5 %all-gather.2.cloned.1.call-done = bf16[512,2048]{1,0:T(8,128)(2,1)} async-done(((bf16[64,2048]{1,0:T(8,128)(2,1)}), bf16[512,2048]{1,0:T(8,128)(2,1)}) %all-gather.2.cloned.1.call-update) | async-done | bytes 2097168 | tf_op jit(solution)/shard_map/all_gather | solution.py:48
  97.4 2.1 %fusion.1 = f32[512]{0:T(512)S(1)} fusion(bf16[512,2048]{1,0:T(8,128)(2,1)} %all-gather.2.cloned.1.call-done), kind=kLoop, calls=%fused_computation.3 | loop fusion | flops 3145216 | bytes 2099200 | tf_op jit(solution)/shard_map/reduce_sum | solution.py:99
  99.5 4.2 %convolution_convert_fusion = bf16[512,2048]{1,0:T(8,128)(2,1)S(1)} fusion(bf16[256,2048]{1,0:T(8,128)(2,1)S(1)} %copy-done, bf16[2048,256]{1,0:T(8,128)(2,1)} %param.22, bf16[512,2048]{1,0:T(8,128)(2,1)} %all-gather.2.cloned.1.call-done, f32[2048]{0:T(1024)S(1)} %convert_element_type.83, f32[512]{0:T(512)S(1)} %add_rsqrt_fusion), kind=kOutput, calls=%fused_computation.7 | convolution fusion | flops 1078460416 | bytes 6301696 | tf_op jit(solution)/shard_map/dot_general | solution.py:137
  103.7 50.8 %all_to_all.34 = bf16[32,16,2048]{2,1,0:T(8,128)(2,1)S(1)} all-to-all(bf16[32,16,2048]{2,1,0:T(8,128)(2,1)S(1)} %bitcast.44), channel_id=1, replica_groups=mesh['kv_0'=8,'kv_1'=4,'tp'=8] {'kv_0','kv_1'}, dimensions={0} | all-to-all | bytes 4194304 | tf_op jit(solution)/shard_map/all_to_all | solution.py:41
  154.4 0.3 convert_reduce_fusion
  154.8 16.1 %all_to_all.35 = bf16[16,8,256]{2,0,1:T(8,128)(2,1)S(1)} all-to-all(bf16[16,8,256]{2,0,1:T(8,128)(2,1)S(1)} %bitcast.50), channel_id=1, replica_groups=mesh['kv_0'=8,'kv_1'=4,'tp'=8] {'tp'}, dimensions={1} | all-to-all | bytes 131072 | tf_op jit(solution)/shard_map/all_to_all | solution.py:140
  170.9 0.6 copy.68
  (35 shorter events, 1.9 us)
Async XLA Ops:
  7.2 92.3 %copy-start = (bf16[256,2048]{1,0:T(8,128)(2,1)S(1)}, bf16[256,2048]{1,0:T(8,128)(2,1)}, u32[]{:S(2)}) copy-start(bf16[256,2048]{1,0:T(8,128)(2,1)} %param.23) | copy-start | bytes 3145732
  8.9 16.0 %all-to-all-start = ((bf16[8,128,256]{2,1,0:T(8,128)(2,1)}), bf16[8,128,256]{2,1,0:T(8,128)(2,1)S(1)}, u32[]{:S(2)}, u32[]{:S(2)}) async-start(bf16[8,128,256]{2,1,0:T(8,128)(2,1)} %broadcast_in_dim.2), calls=%async_computation | async-start | bytes 1048576 | tf_op jit(solution)/shard_map/all_to_all | solution.py:24
  25.2 3.0 %copy-start.1 = (f32[128,2,64,64]{0,3,2,1:T(8,128)S(1)}, f32[128,2,64,64]{0,3,2,1:T(8,128)}, u32[]{:S(2)}) copy-start(f32[128,2,64,64]{0,3,2,1:T(8,128)} %param.13) | copy-start | bytes 12582916
  28.2 3.4 %copy-start.2 = (bf16[128,2048]{1,0:T(8,128)(2,1)S(1)}, bf16[128,2048]{1,0:T(8,128)(2,1)}, u32[]{:S(2)}) copy-start(bf16[128,2048]{1,0:T(8,128)(2,1)} %param.20) | copy-start | bytes 1572868
  28.2 3.4 %copy-start.3 = (bf16[2048,128]{1,0:T(8,128)(2,1)S(1)}, bf16[2048,128]{1,0:T(8,128)(2,1)}, u32[]{:S(2)}) copy-start(bf16[2048,128]{1,0:T(8,128)(2,1)} %param.18) | copy-start | bytes 1572868
  31.4 26.5 %copy-start.4 = (bf16[2048]{0:T(1024)(128)(2,1)S(1)}, bf16[2048]{0:T(1024)(128)(2,1)}, u32[]{:S(2)}) copy-start(bf16[2048]{0:T(1024)(128)(2,1)} %param.21) | copy-start | bytes 12292
  33.4 13.7 %all-to-all-start.1 = ((bf16[8,16,2048]{2,1,0:T(8,128)(2,1)}), bf16[8,16,2048]{2,1,0:T(8,128)(2,1)S(1)}, u32[]{:S(2)}, u32[]{:S(2)}) async-start(bf16[8,16,2048]{2,1,0:T(8,128)(2,1)} %bitcast.14), calls=%async_computation.1 | async-start | bytes 1048576 | tf_op jit(solution)/shard_map/all_to_all | solution.py:41
  37.7 59.7 %all-gather.2.cloned.1.call-start = ((), (), s32[]{:S(2)}) async-start(), calls=%async_computation.4 | async-start | bytes 2359296 | tf_op jit(solution)/shard_map/all_gather | solution.py:48
Sparse Core Ops, SparseCore 0:
  58.0 39.3 all-gather.1
where the time goes:
time: 179 us; the launch traced here: 178 us
  blocking collectives  77.5 us (43%)
  waiting for transfers between devices  51 us (28%)
  between operations  14.2 us (8%)
  starting transfers between devices  10.9 us (6%)
  local copies, waits for them, and re-layouts  9.14 us (5%)
  matrix products  8.12 us (5%)
  other arithmetic  7.33 us (4%)
    all_to_all x1, blocking collectives, summed_on_arrival(): tiles = lax.all_to_all(in_blocks(array, dim, count), axis, 0, 0, tiled=True)  50.8 us
    all_gather x1, waiting for transfers between devices, gathered_by_axis(): nearer = lax.all_gather(array, axes[-1], axis=dim, tiled=True)  39.5 us
    all_to_all x1, blocking collectives, local(): lax.all_to_all(finished, 'tp', split_axis=1, concat_axis=0, tiled=True)  16.1 us
    all_gather x1, blocking collectives, gathered_by_axis(): nearer = lax.all_gather(array, axes[-1], axis=dim, tiled=True)  10.7 us
    all_to_all x1, waiting for transfers between devices, summed_on_arrival(): tiles = lax.all_to_all(in_blocks(array, dim, count), axis, 0, 0, tiled=True)  8.98 us
    all_to_all x1, starting transfers between devices, copy_for_each(): lax.all_to_all(jnp.broadcast_to(array[None], (count, *array.shape)), axis...  6.6 us
    unnamed x15, local copies, waits for them, and re-layouts  5.38 us
    all_to_all x1, starting transfers between devices, summed_on_arrival(): tiles = lax.all_to_all(in_blocks(array, dim, count), axis, 0, 0, tiled=True)  4.34 us
  transfers between devices with their start and end apart: 3, of which 3 were waited for; matrix products, arithmetic and copies ran while one was open for 4% of the time, Pallas kernels for 0%

commit v1 on v0

v1 whole, which is shorter than its diff:
```python
import functools

import jax
import jax.numpy as jnp
from jax import lax
from jax.experimental import pallas as pl
from jax.experimental.pallas import tpu as pltpu
from jax.sharding import Mesh
from jax.sharding import PartitionSpec as P

HEADS = 16
POS = 16384
KV = ("z", "x")
TP = ("y", "c")

EPSILON = 1e-06
ROTARY_BASE = 10000.0

D = 2048
W1 = 768
SIZES = {"z": 8, "x": 4, "y": 4, "c": 2}
F32 = jnp.float32
BF16 = jnp.bfloat16


def slot(offset):
    return 2 * abs(offset) - (1 if offset > 0 else 0)


def last(n):
    return n - 1


class Copies:
    def __init__(self, send_sem, recv_sem):
        self.send_sem, self.recv_sem, self.made = send_sem, recv_sem, []

    def make(self, src, dst, axis, step):
        n = SIZES[axis]
        index = len(self.made)
        copy = pltpu.make_async_remote_copy(
            src_ref=src,
            dst_ref=dst,
            send_sem=self.send_sem.at[index],
            recv_sem=self.recv_sem.at[index],
            device_id={axis: lax.rem(lax.axis_index(axis) + (step + n), n)},
            device_id_type=pl.DeviceIdType.MESH,
        )
        self.made.append(copy)
        return copy

    def send(self, *args):
        copy = self.make(*args)
        copy.start()
        return copy

    def finish(self):
        for copy in self.made:
            copy.wait_send()


def greet(peers):
    barrier = pltpu.get_barrier_semaphore()
    for peer in peers:
        pl.semaphore_signal(barrier, inc=1, device_id=peer, device_id_type=pl.DeviceIdType.MESH)
    return barrier


def neighbour(axis, step):
    n = SIZES[axis]
    return {axis: lax.rem(lax.axis_index(axis) + (step + n), n)}


def half(start, stop, step):
    middle = (start + stop) // 2
    return slice(start, middle) if step > 0 else slice(middle, stop)


def gather_kernel(tok_ref, out_ref, send_sem, recv_sem):
    y, c = lax.axis_index("y"), lax.axis_index("c")
    barrier = greet([neighbour("y", 1), neighbour("y", -1), neighbour("c", 1)])
    out_ref[2 * y + c] = tok_ref[...]
    pl.semaphore_wait(barrier, 3)
    copies = Copies(send_sem, recv_sem)
    rows = tok_ref.shape[0]

    def block(step):
        return 2 * lax.rem(y + (step + 4), 4) + c

    near = {}
    for step in (1, -1):
        near[step] = copies.send(tok_ref, out_ref.at[2 * y + c], "y", step)
    across = [copies.send(tok_ref, out_ref.at[2 * y + c], "c", 1)]
    far = {}
    for step in (1, -1):
        near[step].wait_recv()
        mine = block(-step)
        part = half(0, rows, step)
        far[step] = copies.send(out_ref.at[mine, part], out_ref.at[mine, part], "y", step)
        across.append(copies.send(out_ref.at[mine], out_ref.at[mine], "c", 1))
    for step in (1, -1):
        far[step].wait_recv()
        mine = block(2)
        part = half(0, rows, step)
        across.append(copies.send(out_ref.at[mine, part], out_ref.at[mine, part], "c", 1))
    for copy in across:
        copy.wait_recv()
    copies.finish()


def gather_tokens(tokens):
    rows, width = tokens.shape
    return pl.pallas_call(
        gather_kernel,
        out_shape=jax.ShapeDtypeStruct((8, rows, width), tokens.dtype),
        in_specs=[pl.BlockSpec(memory_space=pltpu.VMEM)],
        out_specs=pl.BlockSpec(memory_space=pltpu.VMEM),
        scratch_shapes=[pltpu.SemaphoreType.DMA((16,)), pltpu.SemaphoreType.DMA((16,))],
        compiler_params=pltpu.CompilerParams(
            collective_id=0, has_side_effects=True, vmem_limit_bytes=4 * 2**20
        ),
        name="gather_tokens",
    )(tokens)


def mixer_kernel(
    part_ref,
    own_ref,
    gain_ref,
    up_hbm,
    down_hbm,
    out_ref,
    up_ref,
    down_ref,
    xs,
    ps,
    pair_in,
    y_sum,
    y_far_in,
    y_near_in,
    mid,
    fin,
    z1_in,
    x1_far_in,
    x1_near_in,
    x2_far_in,
    x2_near_in,
    z2_in,
    load_sem,
    send_sem,
    recv_sem,
):
    y, c = lax.axis_index("y"), lax.axis_index("c")
    tp = 2 * y + c
    peers = [{"y": lax.rem(y + dy, 4), "c": lax.rem(c + dc, 2)} for dy in range(4) for dc in range(2) if dy or dc]
    ring = [neighbour(axis, step) for axis in ("z", "x") for step in (1, -1)]
    barrier = greet(peers + ring)
    load_up = pltpu.make_async_copy(up_hbm, up_ref, load_sem.at[0])
    load_down = pltpu.make_async_copy(down_hbm, down_ref, load_sem.at[1])
    load_up.start()
    load_down.start()
    pl.semaphore_wait(barrier, len(peers) + len(ring))

    copies = Copies(send_sem, recv_sem)
    send = copies.send
    both = (1, -1)

    def rows_for(offset, core):
        return 2 * lax.rem(y + (offset + 4), 4) + core

    offsets = {3: 2, 1: 1, 2: -1, 0: 0}
    across = {}
    for s in (3, 1, 2, 0):
        across[s] = send(part_ref.at[rows_for(offsets[s], 1 - c)], pair_in.at[s], "c", 1)

    def pair_sum(s):
        across[s].wait_recv()
        return part_ref[rows_for(offsets[s], c)].astype(F32) + pair_in[s].astype(F32)

    y_sum[3] = pair_sum(3).astype(BF16)
    far = {}
    for step in both:
        cols = half(0, D, step)
        far[step] = send(y_sum.at[3, :, cols], y_far_in.at[slot(step)], "y", step)
    near = {}
    for step in both:
        s = slot(step)
        cols = half(0, D, step)
        total = pair_sum(s)
        y_sum[s] = total.astype(BF16)
        far[step].wait_recv()
        y_sum[s, :, cols] = (total[:, cols] + y_far_in[s].astype(F32)).astype(BF16)
        near[step] = send(y_sum.at[s], y_near_in.at[s - 1], "y", step)
    attended = pair_sum(0)
    for step in both:
        near[step].wait_recv()
        attended = attended + y_near_in[slot(step) - 1].astype(F32)
    middle = (own_ref[...].astype(F32) + attended).astype(BF16)
    xs[0, 0] = middle
    mid[...] = middle

    c1, c2 = (0, W1), (W1, D)
    full1, full2 = slice(*c1), slice(*c2)
    batches = {"A": slice(0, 1), "B": slice(1, 3), "C": slice(3, 4)}

    def z_hop1(name, step, hop):
        r = batches[name]
        cols = full1 if hop < 4 else half(*c1, step)
        return send(
            xs.at[slot(-step * (hop - 1)), r, :, cols],
            xs.at[slot(-step * hop) if hop < 4 else 7, r, :, cols],
            "z",
            step,
        )

    def z_hop2(step, hop):
        cols = full2 if hop < 4 else half(*c2, step)
        return send(
            xs.at[slot(-step * (hop - 1)), 0, :, cols],
            xs.at[slot(-step * hop) if hop < 4 else 7, 0, :, cols],
            "z",
            step,
        )

    def z_slots(k):
        return slice(0, 1) if k == 0 else slice(7, 8) if k == 4 else slice(2 * k - 1, 2 * k + 1)

    def x_near2(k, step):
        r = z_slots(k)
        return send(xs.at[r, 0, :, full2], xs.at[r, slot(-step), :, full2], "x", step)

    def x_far2(k, step):
        r, cols = z_slots(k), half(*c2, step)
        return send(xs.at[r, slot(-step), :, cols], xs.at[r, 3, :, cols], "x", step)

    x_near1 = {s: send(xs.at[0, 0, :, full1], xs.at[0, slot(-s), :, full1], "x", s) for s in both}
    z2 = {(s, 1): z_hop2(s, 1) for s in both}
    x2n = {(0, s): x_near2(0, s) for s in both}
    z1 = {("A", s, 1): z_hop1("A", s, 1) for s in both}
    x2f = {}

    load_up.wait()
    load_down.wait()

    def mix(k):
        r = z_slots(k)
        n = (r.stop - r.start) * 64
        rows = xs[r].reshape(n, D).astype(F32)
        second_rms = lax.rsqrt(jnp.mean(rows * rows, axis=1, keepdims=True) + EPSILON)
        scaled = (rows * gain_ref[...].astype(F32)).astype(BF16)
        hidden = jnp.dot(scaled, up_ref[...], preferred_element_type=F32) * second_rms
        activated = jnp.square(jnp.maximum(hidden, 0.0)).astype(BF16)
        result = jnp.dot(activated, down_ref[...], preferred_element_type=F32).astype(BF16)
        ps[r] = result.reshape(r.stop - r.start, 4, 16, D)

    x_far1 = {}
    for s in both:
        x_near1[s].wait_recv()
        cols = half(*c1, s)
        x_far1[s] = send(xs.at[0, slot(-s), :, cols], xs.at[0, 3, :, cols], "x", s)
    for s in both:
        z1["B", s, 1] = z_hop1("B", s, 1)

    for level in range(1, 7):
        if level <= 4:
            for s in both:
                z2[s, level].wait_recv()
                if level < 4:
                    z2[s, level + 1] = z_hop2(s, level + 1)
            for s in both:
                x2n[level, s] = x_near2(level, s)
        if level == 2:
            for s in both:
                x_far1[s].wait_recv()
            for s in both:
                z1["C", s, 1] = z_hop1("C", s, 1)
        for name, behind in (("A", 0), ("B", 1), ("C", 2)):
            hop = level - behind
            if 1 <= hop <= 4:
                for s in both:
                    z1[name, s, hop].wait_recv()
                    if hop < 4:
                        z1[name, s, hop + 1] = z_hop1(name, s, hop + 1)
        if level <= 5:
            for s in both:
                x2n[level - 1, s].wait_recv()
                x2f[level - 1, s] = x_far2(level - 1, s)
        if level >= 2:
            for s in both:
                x2f[level - 2, s].wait_recv()
            mix(level - 2)

    def add(index, arrived):
        ps[index] = (ps[index].astype(F32) + arrived.astype(F32)).astype(BF16)

    def x_out_far2(k, s):
        r, cols = z_slots(k), half(*c2, s)
        return send(ps.at[r, 3, :, cols], x2_far_in.at[r, slot(s) - 1], "x", s)

    def x_out_near2(k, s):
        r = z_slots(k)
        return send(ps.at[r, slot(s), :, full2], x2_near_in.at[r, slot(s) - 1], "x", s)

    def z_out1(name, s, hop):
        r = batches[name]
        if hop == 4:
            cols = half(*c1, s)
            return send(ps.at[7, r, :, cols], z1_in.at[slot(s) - 1, 3, r, :, cols], "z", s)
        return send(ps.at[slot(s * hop), r, :, full1], z1_in.at[slot(s) - 1, hop - 1, r, :, full1], "z", s)

    def z_out2(s, hop):
        if hop == 4:
            cols = half(0, D - W1, s)
            return send(ps.at[7, 0, :, half(*c2, s)], z2_in.at[slot(s) - 1, 3, :, cols], "z", s)
        return send(ps.at[slot(s * hop), 0, :, full2], z2_in.at[slot(s) - 1, hop - 1], "z", s)

    def take_far2(k):
        r = z_slots(k)
        for s in both:
            of[k, s].wait_recv()
            add((r, slot(s), slice(None), half(*c2, s)), x2_far_in[r, slot(s) - 1])
            on[k, s] = x_out_near2(k, s)

    def take_near2(k):
        r = z_slots(k)
        for s in both:
            on[k, s].wait_recv()
        arrived = x2_near_in[r, 0].astype(F32) + x2_near_in[r, 1].astype(F32)
        add((r, 0, slice(None), full2), arrived)

    of, on, oz1, oz2 = {}, {}, {}, {}
    for name in ("C", "B", "A"):
        for s in both:
            oz1[name, s, 4] = z_out1(name, s, 4)
    for k in (4, 3, 2):
        for s in both:
            of[k, s] = x_out_far2(k, s)

    def pass_on1(hop):
        for name in ("C", "B", "A"):
            r = batches[name]
            for s in both:
                oz1[name, s, hop + 1].wait_recv()
                cols = half(*c1, s) if hop == 3 else full1
                add((slot(s * hop), r, slice(None), cols), z1_in[slot(s) - 1, hop, r, :, cols])
                oz1[name, s, hop] = z_out1(name, s, hop)

    def pass_on2(hop):
        for s in both:
            oz2[s, hop + 1].wait_recv()
            if hop == 3:
                arrived = z2_in[slot(s) - 1, 3, :, half(0, D - W1, s)]
                add((slot(s * 3), 0, slice(None), half(*c2, s)), arrived)
            else:
                add((slot(s * hop), 0, slice(None), full2), z2_in[slot(s) - 1, hop])
            oz2[s, hop] = z_out2(s, hop)

    take_far2(4)
    pass_on1(3)
    take_far2(3)
    for k in (1, 0):
        for s in both:
            of[k, s] = x_out_far2(k, s)
    take_near2(4)
    for s in both:
        oz2[s, 4] = z_out2(s, 4)
    pass_on1(2)
    take_near2(3)
    take_far2(2)
    pass_on2(3)
    pass_on1(1)
    take_near2(2)
    take_far2(1)
    pass_on2(2)
    for name in ("C", "B", "A"):
        r = batches[name]
        for s in both:
            oz1[name, s, 1].wait_recv()
        arrived = z1_in[0, 0, r, :, full1].astype(F32) + z1_in[1, 0, r, :, full1].astype(F32)
        add((0, r, slice(None), full1), arrived)
        if name == "C":
            far1 = {}
            for s in both:
                far1[s] = send(ps.at[0, 3, :, half(*c1, s)], x1_far_in.at[slot(s) - 1], "x", s)
    take_near2(1)
    take_far2(0)
    pass_on2(1)
    near1 = {}
    for s in both:
        far1[s].wait_recv()
        add((0, slot(s), slice(None), half(*c1, s)), x1_far_in[slot(s) - 1])
        near1[s] = send(ps.at[0, slot(s), :, full1], x1_near_in.at[slot(s) - 1], "x", s)
    take_near2(0)
    down2 = ps[0, 0, :, full2].astype(F32)
    for s in both:
        oz2[s, 1].wait_recv()
        down2 = down2 + z2_in[slot(s) - 1, 0].astype(F32)
    down1 = ps[0, 0, :, full1].astype(F32)
    for s in both:
        near1[s].wait_recv()
        down1 = down1 + x1_near_in[slot(s) - 1].astype(F32)
    fin[:, full2] = (mid[:, full2].astype(F32) + down2).astype(BF16)
    fin[:, full1] = (mid[:, full1].astype(F32) + down1).astype(BF16)

    width = out_ref.shape[2]

    def features(index):
        return pl.ds(pl.multiple_of(index * width, width), width)

    back = []
    index = len(copies.made)
    for peer in peers:
        other = 2 * peer["y"] + peer["c"]
        copy = pltpu.make_async_remote_copy(
            src_ref=fin.at[:, features(other)],
            dst_ref=out_ref.at[tp],
            send_sem=send_sem.at[index],
            recv_sem=recv_sem.at[index],
            device_id=peer,
            device_id_type=pl.DeviceIdType.MESH,
        )
        copy.start()
        back.append(copy)
        index += 1
    out_ref[tp] = fin[:, features(tp)]
    for copy in back:
        copy.wait_recv()
    for copy in back:
        copy.wait_send()
    copies.finish()


def mix_channels(partial, own_rows, channel_gain, w_up, w_down):
    vmem = pl.BlockSpec(memory_space=pltpu.VMEM)
    anywhere = pl.BlockSpec(memory_space=pl.ANY)
    hidden = w_up.shape[1]
    w2 = D - W1
    copies = 160
    return pl.pallas_call(
        mixer_kernel,
        out_shape=jax.ShapeDtypeStruct((8, 16, 256), BF16),
        in_specs=[vmem, vmem, vmem, anywhere, anywhere],
        out_specs=vmem,
        scratch_shapes=[
            pltpu.VMEM((D, hidden), BF16),
            pltpu.VMEM((hidden, D), BF16),
            pltpu.VMEM((8, 4, 16, D), BF16),
            pltpu.VMEM((8, 4, 16, D), BF16),
            pltpu.VMEM((4, 16, D), BF16),
            pltpu.VMEM((4, 16, D), BF16),
            pltpu.VMEM((3, 16, D // 2), BF16),
            pltpu.VMEM((2, 16, D), BF16),
            pltpu.VMEM((16, D), BF16),
            pltpu.VMEM((16, D), BF16),
            pltpu.VMEM((2, 4, 4, 16, W1), BF16),
            pltpu.VMEM((2, 16, W1 // 2), BF16),
            pltpu.VMEM((2, 16, W1), BF16),
            pltpu.VMEM((8, 2, 16, w2 // 2), BF16),
            pltpu.VMEM((8, 2, 16, w2), BF16),
            pltpu.VMEM((2, 4, 16, w2), BF16),
            pltpu.SemaphoreType.DMA((2,)),
            pltpu.SemaphoreType.DMA((copies,)),
            pltpu.SemaphoreType.DMA((copies,)),
        ],
        compiler_params=pltpu.CompilerParams(
            collective_id=1, has_side_effects=True, vmem_limit_bytes=40 * 2**20
        ),
        name="mix_channels",
    )(partial.reshape(8, 16, D), own_rows, channel_gain.reshape(1, D), w_up, w_down)


def rotate(vectors):
    half_size = vectors.shape[-1] // 2
    frequency = ROTARY_BASE ** (-jnp.arange(half_size, dtype=F32) / half_size)
    angles = POS * frequency
    cosine = jnp.cos(angles)
    sines = jnp.sin(angles)
    first_half = vectors[..., :half_size]
    second = vectors[..., half_size:]
    return jnp.concatenate(
        [first_half * cosine - second * sines, first_half * sines + second * cosine], axis=-1
    )


def retain(normed, states, w_query, w_key, w_value, w_gate, head_gain, head_ids):
    row_count = states.shape[0]
    head_count = states.shape[1]
    head_size = states.shape[2]

    def project(weight):
        return jnp.dot(normed, weight, preferred_element_type=F32).reshape(
            row_count, head_count, head_size
        )

    queries = rotate(project(w_query)) * head_size ** (-0.5)
    keys_now = rotate(project(w_key))
    values = project(w_value)
    gating = jnp.dot(normed, w_gate, preferred_element_type=F32)
    decays = 1.0 - jnp.exp2(-1.0 - 11.0 * head_ids / (HEADS - 1))
    new_states = (
        decays[None, :, None, None] * states + keys_now[:, :, :, None] * values[:, :, None, :]
    )
    output = jnp.einsum("bhk,bhkv->bhv", queries, new_states, precision=lax.Precision.HIGHEST)
    center = output - jnp.mean(output, axis=-1, keepdims=True)
    spread = jnp.mean(center * center, axis=-1, keepdims=True)
    scaled = (
        center
        * lax.rsqrt(spread + EPSILON)
        * head_gain.astype(F32).reshape(head_count, head_size)
    )
    gated_out = (scaled.reshape(row_count, head_count * head_size) * jax.nn.silu(gating)).astype(
        BF16
    )
    return (gated_out, new_states)


def local(
    tokens,
    states,
    mix_gain,
    w_query,
    w_key,
    w_value,
    w_gate,
    head_gain,
    w_output,
    channel_gain,
    w_up,
    w_down,
):
    blocks = gather_tokens(tokens)
    full_rows = jnp.moveaxis(blocks, 0, 1).reshape(tokens.shape[0], D)
    widened = full_rows.astype(F32)
    inverse_rms = lax.rsqrt(jnp.mean(widened * widened, axis=1, keepdims=True) + EPSILON)
    normed = (widened * inverse_rms * mix_gain.astype(F32)).astype(BF16)
    local_heads = states.shape[1]
    tp_index = lax.axis_index(TP)
    head_ids = (tp_index * local_heads + jnp.arange(local_heads)).astype(F32)
    gated_out, new_states = retain(
        normed, states, w_query, w_key, w_value, w_gate, head_gain, head_ids
    )
    partial_value = jnp.dot(gated_out, w_output, preferred_element_type=F32).astype(BF16)
    own_rows = lax.dynamic_slice_in_dim(full_rows, tp_index * 16, 16, 0)
    out = mix_channels(partial_value, own_rows, channel_gain, w_up, w_down)
    return (out.reshape(128, 256), new_states)


def solution(mesh):
    torus = Mesh(mesh.devices.reshape(8, 4, 4, 2), ("z", "x", "y", "c"))
    in_specs = (
        P(KV, TP),
        P(KV, TP, None, None),
        P(),
        P(None, TP),
        P(None, TP),
        P(None, TP),
        P(None, TP),
        P(TP),
        P(TP, None),
        P(),
        P(None, KV),
        P(KV, None),
    )
    out_specs = (P(KV, TP), P(KV, TP, None, None))
    return jax.shard_map(local, mesh=torus, in_specs=in_specs, out_specs=out_specs, check_vma=False)
```

time: 179 us -> 96.4 us (0.54)
  Pallas kernels: 0 us -> 80.3 us
  blocking collectives: 77.5 us -> 0 us
  waiting for transfers between devices: 51 us -> 0 us
  between operations: 14.2 us -> 0.88 us
  starting transfers between devices: 10.9 us -> 0 us
  matrix products: 8.12 us -> 2.68 us
  local copies, waits for them, and re-layouts: 9.14 us -> 6.09 us
    pallas_call x0 -> x2, Pallas kernels: none -> 80.3 us  [the longest x1 68.6 us: mix_channels(): pl.pallas_call(mixer_kernel, out_shape=jax.ShapeDtypeStruct((8, 16, 256),...]
    all_to_all x2 -> x0, blocking collectives: 66.9 us -> none  [the longest x1 50.8 us: summed_on_arrival(): tiles = lax.all_to_all(in_blocks(array, dim, count), axis, 0, 0, tiled=True)]
    all_gather x1 -> x0, waiting for transfers between devices: 39.5 us -> none  [gathered_by_axis(): nearer = lax.all_gather(array, axes[-1], axis=dim, tiled=True)]
    all_to_all x2 -> x0, waiting for transfers between devices: 11.6 us -> none  [the longest x1 8.98 us: summed_on_arrival(): tiles = lax.all_to_all(in_blocks(array, dim, count), axis, 0, 0, tiled=True)]
    all_to_all x2 -> x0, starting transfers between devices: 10.9 us -> none  [the longest x1 6.6 us: copy_for_each(): lax.all_to_all(jnp.broadcast_to(array[None], (count, *array.shape)), axis...]
    all_gather x1 -> x0, blocking collectives: 10.7 us -> none  [gathered_by_axis(): nearer = lax.all_gather(array, axes[-1], axis=dim, tiled=True)]
    dot_general x5 -> x4, matrix products: 8.12 us -> 2.68 us  [the longest x1 1.81 us: local(): jnp.dot(gated_out, w_output, preferred_element_type=F32).astype(BF16)]
    reduce_sum x3 -> x0, other arithmetic: 2.47 us -> none  [the longest x1 2.07 us: activate(): jnp.mean(spread_rows * spread_rows, axis=1, keepdims=True) + EPSILON]
  transfers between devices with their start and end apart: 3 -> 0, of which waited for: 3 -> 0; matrix products, arithmetic and copies ran while one was open for 4% -> 0% of each run, Pallas kernels for 0% -> 0%
where the time goes in v1:
time: 96.4 us; the launch traced here: 96.1 us
  Pallas kernels  80.3 us (83%)
  other arithmetic  6.21 us (6%)
  local copies, waits for them, and re-layouts  6.09 us (6%)
  matrix products  2.68 us (3%)
    pallas_call x1, Pallas kernels, mix_channels(): pl.pallas_call(mixer_kernel, out_shape=jax.ShapeDtypeStruct((8, 16, 256),...  68.6 us
    pallas_call x1, Pallas kernels, gather_tokens(): pl.pallas_call(gather_kernel, out_shape=jax.ShapeDtypeStruct((8, rows, wi...  11.7 us
    dot_general x1, other arithmetic, retain(): jnp.einsum('bhk,bhkv->bhv', queries, new_states, precision=lax.Precision....  5.46 us
    unnamed x22, local copies, waits for them, and re-layouts  3.25 us

profile of v1, /device:TPU:1, one launch (start us, length us, event | category | flops | bytes accessed | tf_op | source)
XLA Modules:
  0.0 96.1 jit_solution(7203905127377886646)
XLA Ops:
  0.6 0.0 copy-start
  0.7 0.9 copy-done.3
  1.5 11.7 %gather_tokens.1 = bf16[8,128,256]{2,1,0:T(8,128)(2,1)S(1)} custom-call(bf16[128,256]{1,0:T(8,128)(2,1)S(1)} %copy-done.3), custom_call_target="tpu_custom_call" | custom-call | tf_op jit(solution)/shard_map/gather_tokens/pallas_call | solution.py:113
  13.3 0.2 fusion
  13.5 0.7 mul.197
  14.2 0.2 fusion.2
  14.4 0.3 copy.18
  14.6 1.2 %copy.19 = bf16[2048,128]{0,1:T(8,128)(2,1)S(1)} copy(bf16[2048,128]{1,0:T(8,128)(2,1)} %param.15) | data formatting | bytes 1048576 | tf_op args[3]
  15.9 0.3 fusion.10
  16.2 0.2 copy.21
  16.4 0.3 fusion.11
  16.8 0.1 fusion.8
  16.8 0.1 multiply_subtract_fusion
  16.9 0.2 copy.23
  17.2 0.3 fusion.12
  17.5 5.5 %multiply_reduce_fusion = (f32[128,2,64]{0,2,1:T(8,128)S(1)}, f32[128,2,64,64]{0,3,2,1:T(8,128)}) fusion(f32[128,2,64]{0,2,1:T(8,128)S(1)} %get-tuple-element.10, f32[128,2,64]{0,2,1:T(8,128)S(1)} %fusion.12, f32[128,2,64]{0,2,1:T(8,128)S(1)} %get-tuple-element.11, f32[128,2,64,64]{0,3,2,1:T(8,128)} %param.13, f32[2]{0:T(128)S(1)} %exponential_subtract_fusion), kind=kLoop, calls=%fused_computation | loop fusion | flops 5226496 | bytes 8650760 | tf_op jit(solution)/shard_map/bhk,bhkv->bhv/dot_general | solution.py:503
  23.1 0.1 reshape.111
  23.2 0.1 multiply_multiply_fusion
  23.3 0.1 copy.26
  23.4 0.8 copy.39
  24.2 1.8 %convolution_convert_fusion = bf16[128,2048]{1,0:T(8,128)(2,1)S(1)} fusion(bf16[128,2048]{1,0:T(8,128)(2,1)S(1)} %copy-done, f32[128,128]{1,0:T(8,128)S(1)} %copy.26, bf16[2048,128]{1,0:T(8,128)(2,1)} %param.18, bf16[128,2048]{1,0:T(8,128)(2,1)} %bitcast.36, f32[2048]{0:T(1024)S(1)} %convert_element_type.37, f32[128]{0:T(128)S(1)} %add_rsqrt_fusion.1), kind=kOutput, calls=%fused_computation.2 | convolution fusion | flops 135626752 | bytes 2171392 | tf_op jit(solution)/shard_map/dot_general | solution.py:542
  26.0 0.8 constant_dynamic-slice_fusion.own_ref
  26.9 68.6 %mix_channels.1 = bf16[8,16,256]{2,1,0:T(8,128)(2,1)S(1)} custom-call(bf16[8,16,2048]{2,1,0:T(8,128)(2,1)S(1)} %bitcast.31, bf16[16,2048]{1,0:T(8,128)(2,1)S(1)} %constant_dynamic-slice_fusion.own_ref, bf16[1,2048]{1,0:T(2,128)(2,1)S(1)} %reshape.109.gain_ref, bf16[2048,256]{1,0:T(8,128)(2,1)S(1)} %copy-done.1, bf16[256,2048]{1,0:T(8,128)(2,1)S(1)} %copy-done.2), custom_call_target="tpu_custom_call" | custom-call | tf_op jit(solution)/shard_map/mix_channels/pallas_call | solution.py:439
  95.5 0.6 copy.41
  (26 shorter events, 0.2 us)
Async XLA Ops:
  0.6 23.6 %copy-start = (bf16[128,2048]{1,0:T(8,128)(2,1)S(1)}, bf16[128,2048]{1,0:T(8,128)(2,1)}, u32[]{:S(2)}) copy-start(bf16[128,2048]{1,0:T(8,128)(2,1)} %param.20) | copy-start | bytes 1572868
  0.6 0.9 copy-start.3
  1.5 14.6 %copy-start.4 = (bf16[2048,128]{1,0:T(8,128)(2,1)S(1)}, bf16[2048,128]{1,0:T(8,128)(2,1)}, u32[]{:S(2)}) copy-start(bf16[2048,128]{1,0:T(8,128)(2,1)} %param.16) | copy-start | bytes 1572868
  1.5 15.4 %copy-start.5 = (bf16[2048,128]{1,0:T(8,128)(2,1)S(1)}, bf16[2048,128]{1,0:T(8,128)(2,1)}, u32[]{:S(2)}) copy-start(bf16[2048,128]{1,0:T(8,128)(2,1)} %param.17) | copy-start | bytes 1572868
  17.5 5.6 %copy-start.8 = (bf16[128]{0:T(256)(128)(2,1)S(1)}, bf16[128]{0:T(256)(128)(2,1)}, u32[]{:S(2)}) copy-start(bf16[128]{0:T(256)(128)(2,1)} %param.19) | copy-start | bytes 772
  17.5 6.7 %copy-start.6 = (bf16[2048]{0:T(1024)(128)(2,1)S(1)}, bf16[2048]{0:T(1024)(128)(2,1)}, u32[]{:S(2)}) copy-start(bf16[2048]{0:T(1024)(128)(2,1)} %param.14) | copy-start | bytes 12292
  17.5 9.4 %copy-start.7 = (bf16[2048]{0:T(1024)(128)(2,1)S(1)}, bf16[2048]{0:T(1024)(128)(2,1)}, u32[]{:S(2)}) copy-start(bf16[2048]{0:T(1024)(128)(2,1)} %param.21) | copy-start | bytes 12292
  17.5 9.4 %copy-start.1 = (bf16[2048,256]{1,0:T(8,128)(2,1)S(1)}, bf16[2048,256]{1,0:T(8,128)(2,1)}, u32[]{:S(2)}) copy-start(bf16[2048,256]{1,0:T(8,128)(2,1)} %up_hbm.1) | copy-start | bytes 3145732
  17.5 9.4 %copy-start.2 = (bf16[256,2048]{1,0:T(8,128)(2,1)S(1)}, bf16[256,2048]{1,0:T(8,128)(2,1)}, u32[]{:S(2)}) copy-start(bf16[256,2048]{1,0:T(8,128)(2,1)} %down_hbm.1) | copy-start | bytes 3145732

commit v2 on v0

v2 whole, which is shorter than its diff:
```python
import jax
import jax.numpy as jnp
import numpy as np
from jax import lax
from jax.experimental import pallas as pl
from jax.experimental.pallas import tpu as pltpu
from jax.sharding import Mesh
from jax.sharding import PartitionSpec as P

HEADS = 16
POS = 16384
KV = ("z", "x")
TP = ("y", "c")

EPSILON = 1e-06
ROTARY_BASE = 10000.0

D = 2048
SIZES = {"z": 8, "x": 4, "y": 4, "c": 2}
F32 = jnp.float32
BF16 = jnp.bfloat16


def slot(offset):
    return 2 * abs(offset) - (1 if offset > 0 else 0)


class Copies:
    def __init__(self, send_sem, recv_sem):
        self.send_sem, self.recv_sem, self.made = send_sem, recv_sem, []

    def send_to(self, src, dst, device):
        index = len(self.made)
        copy = pltpu.make_async_remote_copy(
            src_ref=src,
            dst_ref=dst,
            send_sem=self.send_sem.at[index],
            recv_sem=self.recv_sem.at[index],
            device_id=device,
            device_id_type=pl.DeviceIdType.MESH,
        )
        copy.start()
        self.made.append(copy)
        return copy

    def send(self, src, dst, axis, step):
        return self.send_to(src, dst, neighbour(axis, step))

    def finish(self):
        for copy in self.made:
            copy.wait_send()


def greet(peers):
    barrier = pltpu.get_barrier_semaphore()
    for peer in peers:
        pl.semaphore_signal(barrier, inc=1, device_id=peer, device_id_type=pl.DeviceIdType.MESH)
    return barrier


def neighbour(axis, step):
    n = SIZES[axis]
    return {axis: lax.rem(lax.axis_index(axis) + (step + n), n)}


def half(start, stop, step):
    middle = (start + stop) // 2
    return slice(start, middle) if step > 0 else slice(middle, stop)


def layer_kernel(
    tok_hbm,
    states_hbm,
    mix_gain_hbm,
    wq_hbm,
    wk_hbm,
    wv_hbm,
    wg_hbm,
    head_gain_hbm,
    wo_hbm,
    channel_gain_hbm,
    up_hbm,
    down_hbm,
    turn_hbm,
    out_ref,
    new_ref,
    mix_gain_ref,
    head_gain_ref,
    channel_gain_ref,
    turn_ref,
    blocks,
    w_ref,
    wo_ref,
    states,
    normed,
    q_t,
    k_t,
    gated_t,
    part,
    up_ref,
    down_ref,
    up_far,
    down_far,
    xs,
    ps,
    scaled,
    pair_in,
    y_sum,
    y_in,
    mid,
    fin,
    x_in,
    z3_in,
    z4_in,
    z_in,
    load_sem,
    state_sem,
    send_sem,
    recv_sem,
):
    x, y, c = lax.axis_index("x"), lax.axis_index("y"), lax.axis_index("c")
    tp = 2 * y + c
    both = (1, -1)
    mate = {"x": lax.rem(x + 1 + 2 * lax.rem(x + c, 2), 4)}
    peers = [{"y": lax.rem(y + dy, 4), "c": lax.rem(c + dc, 2)} for dy in range(4) for dc in range(2) if dy or dc]
    ring = [neighbour("z", step) for step in (1, -1, 2, -2)] + [mate, neighbour("x", 2)]
    barrier = greet(peers + ring)

    heads, size = states.shape[0], states.shape[1]
    chunk = 16
    spans = [(h, slice(k, k + chunk)) for h in range(heads) for k in range(0, size, chunk)]
    load_tok = pltpu.make_async_copy(tok_hbm, blocks.at[tp], load_sem.at[0])
    load_up = pltpu.make_async_copy(up_hbm, up_ref, load_sem.at[1])
    load_down = pltpu.make_async_copy(down_hbm, down_ref, load_sem.at[2])
    load_w = []
    for i, w in enumerate((wq_hbm, wk_hbm, wv_hbm, wg_hbm)):
        load_w.append(pltpu.make_async_copy(w, w_ref.at[:, 128 * i : 128 * (i + 1)], load_sem.at[3 + i]))
    load_out = pltpu.make_async_copy(wo_hbm, wo_ref, load_sem.at[7])
    load_states = []
    for i, (h, k) in enumerate(spans):
        load_states.append(pltpu.make_async_copy(states_hbm.at[h, k], states.at[h, k], state_sem.at[i]))
    small = ((mix_gain_hbm, mix_gain_ref), (head_gain_hbm, head_gain_ref), (channel_gain_hbm, channel_gain_ref), (turn_hbm, turn_ref))
    load_small = [pltpu.make_async_copy(src, dst, load_sem.at[8 + i]) for i, (src, dst) in enumerate(small)]
    for copy in [load_tok, load_up, load_down] + load_small + load_w + load_states + [load_out]:
        copy.start()
    load_tok.wait()
    pl.semaphore_wait(barrier, len(peers) + len(ring))

    copies = Copies(send_sem, recv_sem)
    send = copies.send

    own = blocks.at[tp]
    near = {step: send(own, own, "y", step) for step in (2, 1, -1)}
    across = [send(own, own, "c", 1)]

    load_up.wait()
    load_down.wait()
    weights = []
    for held, far in ((up_ref, up_far), (down_ref, down_far)):
        deep = held.shape[0] // 4
        for i in range(2):
            rows = pl.ds(pl.multiple_of((2 * c + i) * deep, deep), deep)
            weights.append((far.at[rows], send(held.at[rows], far.at[rows], "x", 2)))
    handed = []

    def hand_over(i):
        there, copy = weights[i]
        copy.wait_recv()
        handed.append(send(there, there, "c", 1))

    for step in (1, -1, 2):
        near[step].wait_recv()
        arrived = blocks.at[2 * lax.rem(y + (4 - step), 4) + c]
        across.append(send(arrived, arrived, "c", 1))
    for copy in across:
        copy.wait_recv()

    for copy in load_small:
        copy.wait()
    width = blocks.shape[2]
    lanes = 128
    mix_gain = mix_gain_ref[...].astype(F32)
    total = 0.0
    for i in range(8):
        block = blocks[i].astype(F32)
        total = total + jnp.sum(block * block, axis=1, keepdims=True)
    inverse_rms = lax.rsqrt(total / D + EPSILON)
    for i in range(D // lanes):
        off = i * lanes % width
        block = blocks[i * lanes // width, :, off : off + lanes].astype(F32)
        normed[:, i * lanes : (i + 1) * lanes] = (block * inverse_rms * mix_gain[i : i + 1]).astype(BF16)
    for copy in load_w:
        copy.wait()
    projected = jnp.dot(normed[...], w_ref[...], preferred_element_type=F32)

    turned = [projected[:, 128 * i : 128 * (i + 1)].T for i in range(4)]
    cosine, sines = turn_ref[0 : size // 2], turn_ref[size // 2 : size]
    for source, target, scale in ((turned[0], q_t, size ** (-0.5)), (turned[1], k_t, 1.0)):
        for h in range(heads):
            first = source[h * size : h * size + size // 2]
            second = source[h * size + size // 2 : (h + 1) * size]
            target[h * size : h * size + size // 2] = (first * cosine - second * sines) * scale
            target[h * size + size // 2 : (h + 1) * size] = (first * sines + second * cosine) * scale
    for h in range(heads):
        head = jnp.full((1, lanes), heads * tp + h).astype(F32)
        decay = 1.0 - jnp.exp2(-1.0 - 11.0 * head / (HEADS - 1))
        rows = slice(h * size, (h + 1) * size)
        values = turned[2][rows]
        output = jnp.zeros_like(values)
        for i, (span_head, ks) in enumerate(spans):
            if span_head != h:
                continue
            load_states[i].wait()

            def step(j, output):
                for u in range(4):
                    k = ks.start + 4 * j + u
                    row = h * size + k
                    new = decay * states[h, k] + k_t[pl.ds(row, 1)] * values
                    new_ref[h, k] = new
                    output = output + q_t[pl.ds(row, 1)] * new
                return output

            output = lax.fori_loop(0, chunk // 4, step, output)
        center = output - jnp.mean(output, axis=0, keepdims=True)
        spread = jnp.mean(center * center, axis=0, keepdims=True)
        gate = turned[3][rows]
        gated_t[rows] = center * lax.rsqrt(spread + EPSILON) * (gate * jax.nn.sigmoid(gate))
    gated = (gated_t[...].T * head_gain_ref[...].astype(F32)).astype(BF16)
    load_out.wait()
    part[...] = jnp.dot(gated, wo_ref[...], preferred_element_type=F32).astype(BF16).reshape(8, 16, D)

    def rows_for(offset, core):
        return 2 * lax.rem(y + (offset + 4), 4) + core

    offsets = (2, 1, -1, 0)
    across = [send(part.at[rows_for(o, 1 - c)], pair_in.at[i], "c", 1) for i, o in enumerate(offsets)]

    def pair_sum(i):
        across[i].wait_recv()
        return part[rows_for(offsets[i], c)].astype(F32) + pair_in[i].astype(F32)

    near = []
    for i in range(3):
        y_sum[i] = pair_sum(i).astype(BF16)
        near.append(send(y_sum.at[i], y_in.at[i], "y", offsets[i]))
    attended = pair_sum(3)
    hand_over(0)
    mine = pl.ds(pl.multiple_of(16 * tp, 16), 16)
    own_rows = jnp.concatenate([blocks[i, mine] for i in range(8)], axis=1).astype(F32)
    for i in (1, 2, 0):
        near[i].wait_recv()
        attended = attended + y_in[i].astype(F32)
    middle = (own_rows + attended).astype(BF16)
    xs[0, 0] = middle
    mid[...] = middle

    z1, z2, z3, z4, xn = {}, {}, {}, {}, {}

    def to_mate(s):
        xn[s] = copies.send_to(xs.at[s, 0], xs.at[s, 1], mate)

    def halves(s):
        return (0, 1) if s > 0 else (1, 0)

    def side(h):
        return slice(h * D // 2, (h + 1) * D // 2)

    for i in range(2):
        for s in both:
            cols = side(halves(s)[i])
            z2[s, i] = send(xs.at[0, 0, :, cols], xs.at[slot(-2 * s), 0, :, cols], "z", 2 * s)
    for s in both:
        z1[s] = send(xs.at[0, 0], xs.at[slot(-s), 0], "z", s)
    to_mate(0)
    hand_over(1)
    for i in range(2):
        for s in both:
            z2[s, i].wait_recv()
            came = slot(-2 * s)
            cols = side(halves(s)[i])
            if i == 0:
                z4[s] = send(xs.at[came, 0, :, cols], xs.at[7, 0, :, cols], "z", 2 * s)
            z3[s, i] = send(xs.at[came, 0, :, cols], xs.at[slot(-3 * s), 0, :, cols], "z", s)
            if i == 1:
                to_mate(came)
    for s in both:
        z1[s].wait_recv()
        to_mate(slot(-s))
    for s in both:
        z4[s].wait_recv()
    to_mate(7)
    for s in both:
        for i in range(2):
            z3[s, i].wait_recv()
        to_mate(slot(-3 * s))
    hand_over(2)
    hand_over(3)

    gain = channel_gain_ref[...].astype(F32)

    def mix(first, stop):
        n = (stop - first) * 32
        squares = 0.0
        for i in range(D // lanes):
            cols = slice(i * lanes, (i + 1) * lanes)
            rows = xs[first:stop, :, :, cols].reshape(n, lanes).astype(F32)
            squares = squares + rows * rows
            scaled[0:n, cols] = (rows * gain[i : i + 1]).astype(BF16)
        second_rms = lax.rsqrt(jnp.sum(squares, axis=1, keepdims=True) / D + EPSILON)
        result = 0.0
        for up, down in ((up_ref, down_ref), (up_far, down_far)):
            hidden = jnp.dot(scaled[0:n], up[...], preferred_element_type=F32) * second_rms
            activated = jnp.square(jnp.maximum(hidden, 0.0)).astype(BF16)
            result = result + jnp.dot(activated, down[...], preferred_element_type=F32)
        ps[first:stop] = result.astype(BF16).reshape(stop - first, 2, 16, D)

    for copy in handed:
        copy.wait_recv()
    for s in range(5):
        xn[s].wait_recv()
    mix(0, 5)

    xo = {}

    def back_to_mate(s):
        xo[s] = copies.send_to(ps.at[s, 1], x_in.at[s], mate)

    def with_mate(s):
        xo[s].wait_recv()
        return ps[s, 0].astype(F32) + x_in[s].astype(F32)

    for s in (3, 4, 1, 2, 0):
        back_to_mate(s)
    for s in (7, 5, 6):
        xn[s].wait_recv()
    mix(5, 8)
    for s in (7, 5, 6):
        back_to_mate(s)

    o1, o2, o3, o4 = {}, {}, {}, {}
    ps[7, 0] = with_mate(7).astype(BF16)
    for s in both:
        cols = side(halves(s)[0])
        o4[s] = send(ps.at[7, 0, :, cols], z4_in.at[slot(s) - 1], "z", 2 * s)
    for s in both:
        ps[slot(3 * s), 0] = with_mate(slot(3 * s)).astype(BF16)
    for i in range(2):
        for s in both:
            cols = side(halves(s)[i])
            o3[s, i] = send(ps.at[slot(3 * s), 0, :, cols], z3_in.at[slot(s) - 1, :, cols], "z", s)
    for s in both:
        ps[slot(s), 0] = with_mate(slot(s)).astype(BF16)
        o1[s] = send(ps.at[slot(s), 0], z_in.at[slot(s) - 1], "z", s)
    relayed = {s: with_mate(slot(2 * s)) for s in both}
    for i in range(2):
        for s in both:
            there, cols = slot(2 * s), side(halves(s)[i])
            if i == 0:
                o4[s].wait_recv()
            o3[s, i].wait_recv()
            total = relayed[s][:, cols] + z3_in[slot(s) - 1, :, cols].astype(F32)
            if i == 0:
                total = total + z4_in[slot(s) - 1].astype(F32)
            ps[there, 0, :, cols] = total.astype(BF16)
            o2[s, i] = send(ps.at[there, 0, :, cols], z_in.at[slot(s) + 1, :, cols], "z", 2 * s)
    down_sum = with_mate(0) + mid[...].astype(F32)
    for s in both:
        o1[s].wait_recv()
        down_sum = down_sum + z_in[slot(s) - 1].astype(F32)
    for s in both:
        for i in range(2):
            o2[s, i].wait_recv()
        down_sum = down_sum + z_in[slot(s) + 1].astype(F32)
    fin[...] = down_sum.astype(BF16)

    def features(index):
        return pl.ds(pl.multiple_of(index * width, width), width)

    back = []
    for peer in peers:
        other = 2 * peer["y"] + peer["c"]
        back.append(copies.send_to(fin.at[:, features(other)], out_ref.at[tp], peer))
    out_ref[tp] = fin[:, features(tp)]
    for copy in back:
        copy.wait_recv()
    copies.finish()


def write_kernel(out_vmem, new_vmem, out_hbm, new_hbm, sem):
    copies = [pltpu.make_async_copy(out_vmem, out_hbm, sem.at[0])]
    heads, size = new_vmem.shape[0], new_vmem.shape[1]
    parts = 4
    for h in range(heads):
        for i in range(parts):
            k = slice(i * size // parts, (i + 1) * size // parts)
            copies.append(pltpu.make_async_copy(new_vmem.at[h, k], new_hbm.at[h, k], sem.at[len(copies)]))
    for copy in copies:
        copy.start()
    for copy in copies:
        copy.wait()


def write_out(out, new_states):
    vmem = pl.BlockSpec(memory_space=pltpu.VMEM)
    hbm = pl.BlockSpec(memory_space=pltpu.HBM)
    return pl.pallas_call(
        write_kernel,
        out_shape=(pltpu.HBM(out.shape, out.dtype), pltpu.HBM(new_states.shape, new_states.dtype)),
        in_specs=[vmem, vmem],
        out_specs=(hbm, hbm),
        scratch_shapes=[pltpu.SemaphoreType.DMA((9,))],
        compiler_params=pltpu.CompilerParams(vmem_limit_bytes=8 * 2**20),
        name="write_out",
    )(
        pltpu.with_memory_space_constraint(out, pltpu.VMEM),
        pltpu.with_memory_space_constraint(new_states, pltpu.VMEM),
    )


def in_hbm(array):
    return pltpu.with_memory_space_constraint(array, pltpu.HBM)


def local(
    tokens,
    states,
    mix_gain,
    w_query,
    w_key,
    w_value,
    w_gate,
    head_gain,
    w_output,
    channel_gain,
    w_up,
    w_down,
):
    rows, heads, size, _ = states.shape
    hidden = w_up.shape[1]
    angles = POS * ROTARY_BASE ** (-np.arange(size // 2) / (size // 2))
    turn = np.concatenate([np.cos(angles), np.sin(angles)]).astype(np.float32)[:, None]
    vmem = pl.BlockSpec(memory_space=pltpu.VMEM)
    hbm = pl.BlockSpec(memory_space=pltpu.HBM)
    copies = 80
    out, new_states = pl.pallas_call(
        layer_kernel,
        out_shape=(
            pltpu.VMEM((8, 16, tokens.shape[1]), BF16),
            pltpu.VMEM((heads, size, size, rows), F32),
        ),
        in_specs=[hbm] * 13,
        out_specs=(vmem, vmem),
        scratch_shapes=[
            pltpu.VMEM((D // 128, 128), BF16),
            pltpu.VMEM((1, heads * size), BF16),
            pltpu.VMEM((D // 128, 128), BF16),
            pltpu.VMEM((size, 1), F32),
            pltpu.VMEM((8, rows, tokens.shape[1]), BF16),
            pltpu.VMEM((D, 4 * heads * size), BF16),
            pltpu.VMEM((heads * size, D), BF16),
            pltpu.VMEM((heads, size, size, rows), F32),
            pltpu.VMEM((rows, D), BF16),
            pltpu.VMEM((heads * size, rows), F32),
            pltpu.VMEM((heads * size, rows), F32),
            pltpu.VMEM((heads * size, rows), F32),
            pltpu.VMEM((8, 16, D), BF16),
            pltpu.VMEM((D, hidden), BF16),
            pltpu.VMEM((hidden, D), BF16),
            pltpu.VMEM((D, hidden), BF16),
            pltpu.VMEM((hidden, D), BF16),
            pltpu.VMEM((8, 2, 16, D), BF16),
            pltpu.VMEM((8, 2, 16, D), BF16),
            pltpu.VMEM((160, D), BF16),
            pltpu.VMEM((4, 16, D), BF16),
            pltpu.VMEM((3, 16, D), BF16),
            pltpu.VMEM((3, 16, D), BF16),
            pltpu.VMEM((16, D), BF16),
            pltpu.VMEM((16, D), BF16),
            pltpu.VMEM((8, 16, D), BF16),
            pltpu.VMEM((2, 16, D), BF16),
            pltpu.VMEM((2, 16, D // 2), BF16),
            pltpu.VMEM((4, 16, D), BF16),
            pltpu.SemaphoreType.DMA((12,)),
            pltpu.SemaphoreType.DMA((heads * size // 16,)),
            pltpu.SemaphoreType.DMA((copies,)),
            pltpu.SemaphoreType.DMA((copies,)),
        ],
        compiler_params=pltpu.CompilerParams(
            collective_id=0, has_side_effects=True, vmem_limit_bytes=40 * 2**20
        ),
        name="layer",
    )(
        in_hbm(tokens),
        in_hbm(states.transpose(1, 2, 3, 0)),
        in_hbm(mix_gain.reshape(D // 128, 128)),
        in_hbm(w_query),
        in_hbm(w_key),
        in_hbm(w_value),
        in_hbm(w_gate),
        in_hbm(head_gain.reshape(1, heads * size)),
        in_hbm(w_output),
        in_hbm(channel_gain.reshape(D // 128, 128)),
        in_hbm(w_up),
        in_hbm(w_down),
        in_hbm(jnp.asarray(turn)),
    )
    out, new_states = write_out(out, new_states)
    return (out.reshape(tokens.shape), new_states.transpose(3, 0, 1, 2))


def solution(mesh):
    torus = Mesh(mesh.devices.reshape(8, 4, 4, 2), ("z", "x", "y", "c"))
    in_specs = (
        P(KV, TP),
        P(KV, TP, None, None),
        P(),
        P(None, TP),
        P(None, TP),
        P(None, TP),
        P(None, TP),
        P(TP),
        P(TP, None),
        P(),
        P(None, KV),
        P(KV, None),
    )
    out_specs = (P(KV, TP), P(KV, TP, None, None))
    return jax.shard_map(local, mesh=torus, in_specs=in_specs, out_specs=out_specs, check_vma=False)
```

time: 179 us -> 63.6 us (0.36)
  blocking collectives: 77.5 us -> 0 us
  Pallas kernels: 0 us -> 62.9 us
  waiting for transfers between devices: 51 us -> 0 us
  between operations: 14.2 us -> 0.64 us
  starting transfers between devices: 10.9 us -> 0 us
  local copies, waits for them, and re-layouts: 9.14 us -> 0 us
  matrix products: 8.12 us -> 0 us
  other arithmetic: 7.33 us -> 0 us
    all_to_all x2 -> x0, blocking collectives: 66.9 us -> none  [the longest x1 50.8 us: summed_on_arrival(): tiles = lax.all_to_all(in_blocks(array, dim, count), axis, 0, 0, tiled=True)]
    pallas_call x0 -> x2, Pallas kernels: none -> 62.9 us  [the longest x1 60.8 us: local(): pl.pallas_call(layer_kernel, out_shape=(pltpu.VMEM((8, 16, tokens.shape[1...]
    all_gather x1 -> x0, waiting for transfers between devices: 39.5 us -> none  [gathered_by_axis(): nearer = lax.all_gather(array, axes[-1], axis=dim, tiled=True)]
    all_to_all x2 -> x0, waiting for transfers between devices: 11.6 us -> none  [the longest x1 8.98 us: summed_on_arrival(): tiles = lax.all_to_all(in_blocks(array, dim, count), axis, 0, 0, tiled=True)]
    all_to_all x2 -> x0, starting transfers between devices: 10.9 us -> none  [the longest x1 6.6 us: copy_for_each(): lax.all_to_all(jnp.broadcast_to(array[None], (count, *array.shape)), axis...]
    all_gather x1 -> x0, blocking collectives: 10.7 us -> none  [gathered_by_axis(): nearer = lax.all_gather(array, axes[-1], axis=dim, tiled=True)]
    dot_general x5 -> x0, matrix products: 8.12 us -> none  [the longest x1 4.16 us: local(): jnp.dot(activated, w_down, preferred_element_type=jnp.float32)]
    unnamed x15 -> x0, local copies, waits for them, and re-layouts: 5.38 us -> none
  transfers between devices with their start and end apart: 3 -> 0, of which waited for: 3 -> 0; matrix products, arithmetic and copies ran while one was open for 4% -> 0% of each run, Pallas kernels for 0% -> 0%
where the time goes in v2:
time: 63.6 us; the launch traced here: 63.5 us
  Pallas kernels  62.9 us (99%)
  between operations  0.64 us (1%)
    pallas_call x1, Pallas kernels, local(): pl.pallas_call(layer_kernel, out_shape=(pltpu.VMEM((8, 16, tokens.shape[1...  60.8 us
    pallas_call x1, Pallas kernels, write_out(): pl.pallas_call(write_kernel, out_shape=(pltpu.HBM(out.shape, out.dtype),...  2.1 us

profile of v2, /device:TPU:1, one launch (start us, length us, event | category | flops | bytes accessed | tf_op | source)
XLA Modules:
  0.0 63.5 jit_solution(10039378705545045202)
XLA Ops:
  0.6 60.8 %layer.1 = (bf16[8,16,256]{2,1,0:T(8,128)(2,1)S(1)}, f32[2,64,64,128]{3,2,1,0:T(8,128)S(1)}) custom-call(bf16[128,256]{1,0:T(8,128)(2,1)} %tok_hbm.1, f32[2,64,64,128]{3,2,1,0:T(8,128)} %bitcast.6, bf16[16,128]{1,0:T(8,128)(2,1)} %bitcast.7, bf16[2048,128]{1,0:T(8,128)(2,1)} %wq_hbm.1, bf16[2048,128]{1,0:T(8,128)(2,1)} %wk_hbm.1, bf16[2048,128]{1,0:T(8,128)(2,1)} %wv_hbm.1, ...), custom_call_target="tpu_custom_call" | custom-call | tf_op jit(solution)/shard_map/layer/pallas_call | solution.py:446
  61.4 2.1 %write_out.1 = (bf16[8,16,256]{2,1,0:T(8,128)(2,1)}, f32[2,64,64,128]{3,2,1,0:T(8,128)}) custom-call(bf16[8,16,256]{2,1,0:T(8,128)(2,1)S(1)} %get-tuple-element.6.out_vmem, f32[2,64,64,128]{3,2,1,0:T(8,128)S(1)} %get-tuple-element.7.new_vmem), custom_call_target="tpu_custom_call" | custom-call | tf_op jit(solution)/shard_map/write_out/pallas_call | solution.py:407

commit v3 on v2

--- a/solution.py
+++ b/solution.py
@@ -108,11 +108,10 @@
     y_sum,
     y_in,
     mid,
-    fin,
     x_in,
     z3_in,
     z4_in,
-    z_in,
+    gathered,
     load_sem,
     state_sem,
     send_sem,
@@ -155,12 +154,18 @@
 
     load_up.wait()
     load_down.wait()
+    eighth = down_ref.shape[0] // 8
+
+    def down_rows(step, core):
+        block = 2 * lax.rem(y + (4 - step), 4) + core
+        return down_far.at[pl.ds(pl.multiple_of(block * eighth, eighth), eighth)]
+
+    first_down = send(down_ref.at[pl.ds(pl.multiple_of(tp * eighth, eighth), eighth)], down_rows(0, c), "x", 2)
     weights = []
-    for held, far in ((up_ref, up_far), (down_ref, down_far)):
-        deep = held.shape[0] // 4
-        for i in range(2):
-            rows = pl.ds(pl.multiple_of((2 * c + i) * deep, deep), deep)
-            weights.append((far.at[rows], send(held.at[rows], far.at[rows], "x", 2)))
+    deep = up_ref.shape[0] // 4
+    for i in range(2):
+        rows = pl.ds(pl.multiple_of((2 * c + i) * deep, deep), deep)
+        weights.append((up_far.at[rows], send(up_ref.at[rows], up_far.at[rows], "x", 2)))
     handed = []
 
     def hand_over(i):
@@ -233,60 +238,82 @@
     def rows_for(offset, core):
         return 2 * lax.rem(y + (offset + 4), 4) + core
 
+    def side(h):
+        return slice(h * D // 2, (h + 1) * D // 2)
+
     offsets = (2, 1, -1, 0)
-    across = [send(part.at[rows_for(o, 1 - c)], pair_in.at[i], "c", 1) for i, o in enumerate(offsets)]
-
-    def pair_sum(i):
-        across[i].wait_recv()
-        return part[rows_for(offsets[i], c)].astype(F32) + pair_in[i].astype(F32)
-
-    near = []
-    for i in range(3):
-        y_sum[i] = pair_sum(i).astype(BF16)
-        near.append(send(y_sum.at[i], y_in.at[i], "y", offsets[i]))
-    attended = pair_sum(3)
-    hand_over(0)
+    across, near = {}, {}
+    for h in range(2):
+        for i, o in enumerate(offsets):
+            across[i, h] = send(part.at[rows_for(o, 1 - c), :, side(h)], pair_in.at[i, :, side(h)], "c", 1)
+
+    def pair_sum(i, h):
+        across[i, h].wait_recv()
+        return part[rows_for(offsets[i], c), :, side(h)].astype(F32) + pair_in[i, :, side(h)].astype(F32)
+
+    for h in range(2):
+        for i in range(3):
+            y_sum[i, :, side(h)] = pair_sum(i, h).astype(BF16)
+            near[i, h] = send(y_sum.at[i, :, side(h)], y_in.at[i, :, side(h)], "y", offsets[i])
     mine = pl.ds(pl.multiple_of(16 * tp, 16), 16)
     own_rows = jnp.concatenate([blocks[i, mine] for i in range(8)], axis=1).astype(F32)
-    for i in (1, 2, 0):
-        near[i].wait_recv()
-        attended = attended + y_in[i].astype(F32)
-    middle = (own_rows + attended).astype(BF16)
-    xs[0, 0] = middle
-    mid[...] = middle
-
     z1, z2, z3, z4, xn = {}, {}, {}, {}, {}
+    both_halves = (0, 1)
+    for h in both_halves:
+        attended = pair_sum(3, h)
+        for i in (1, 2, 0):
+            near[i, h].wait_recv()
+            attended = attended + y_in[i, :, side(h)].astype(F32)
+        middle = (own_rows[:, side(h)] + attended).astype(BF16)
+        xs[0, 0, :, side(h)] = middle
+        mid[:, side(h)] = middle
+        for s in both:
+            z2[s, h] = send(xs.at[0, 0, :, side(h)], xs.at[slot(-2 * s), 0, :, side(h)], "z", 2 * s)
 
     def to_mate(s):
         xn[s] = copies.send_to(xs.at[s, 0], xs.at[s, 1], mate)
 
+    def features(index):
+        return pl.ds(pl.multiple_of(index * width, width), width)
+
+    everyone = [{"y": lax.rem(y + dy, 4), "c": lax.rem(c + dc, 2)} for dy in (2, 1, 3, 0) for dc in (1, 0)]
+    spread = []
+
+    def spread_out(row_ref, place, step=0):
+        for peer in everyone if step else everyone[:-1]:
+            other = 2 * peer["y"] + peer["c"]
+            device = dict(peer, **neighbour("z", step)) if step else peer
+            spread.append(copies.send_to(row_ref.at[:, features(other)], gathered.at[place, tp], device))
+        if not step:
+            gathered[place, tp] = row_ref[:, features(tp)]
+
     def halves(s):
         return (0, 1) if s > 0 else (1, 0)
 
-    def side(h):
-        return slice(h * D // 2, (h + 1) * D // 2)
-
-    for i in range(2):
-        for s in both:
-            cols = side(halves(s)[i])
-            z2[s, i] = send(xs.at[0, 0, :, cols], xs.at[slot(-2 * s), 0, :, cols], "z", 2 * s)
     for s in both:
         z1[s] = send(xs.at[0, 0], xs.at[slot(-s), 0], "z", s)
     to_mate(0)
+    first_down.wait_recv()
+    along = {step: send(down_rows(0, c), down_rows(0, c), "y", step) for step in (2, 1, -1)}
+    handed.append(send(down_rows(0, c), down_rows(0, c), "c", 1))
+    hand_over(0)
+    for h in both_halves:
+        for s in both:
+            z2[s, h].wait_recv()
+            came = slot(-2 * s)
+            if h == halves(s)[0]:
+                z4[s] = send(xs.at[came, 0, :, side(h)], xs.at[7, 0, :, side(h)], "z", 2 * s)
+            z3[s, h] = send(xs.at[came, 0, :, side(h)], xs.at[slot(-3 * s), 0, :, side(h)], "z", s)
+            if h == 1:
+                to_mate(came)
     hand_over(1)
-    for i in range(2):
-        for s in both:
-            z2[s, i].wait_recv()
-            came = slot(-2 * s)
-            cols = side(halves(s)[i])
-            if i == 0:
-                z4[s] = send(xs.at[came, 0, :, cols], xs.at[7, 0, :, cols], "z", 2 * s)
-            z3[s, i] = send(xs.at[came, 0, :, cols], xs.at[slot(-3 * s), 0, :, cols], "z", s)
-            if i == 1:
-                to_mate(came)
+    spread_out(mid, 5)
     for s in both:
         z1[s].wait_recv()
         to_mate(slot(-s))
+    for step in (2, 1, -1):
+        along[step].wait_recv()
+        handed.append(send(down_rows(step, c), down_rows(step, c), "c", 1))
     for s in both:
         z4[s].wait_recv()
     to_mate(7)
@@ -294,9 +321,6 @@
         for i in range(2):
             z3[s, i].wait_recv()
         to_mate(slot(-3 * s))
-    hand_over(2)
-    hand_over(3)
-
     gain = channel_gain_ref[...].astype(F32)
 
     def mix(first, stop):
@@ -330,28 +354,36 @@
         xo[s].wait_recv()
         return ps[s, 0].astype(F32) + x_in[s].astype(F32)
 
-    for s in (3, 4, 1, 2, 0):
+    for s in (3, 4):
         back_to_mate(s)
     for s in (7, 5, 6):
         xn[s].wait_recv()
     mix(5, 8)
-    for s in (7, 5, 6):
+    back_to_mate(7)
+    third = {}
+    for i in range(2):
+        for s in both:
+            at, cols = slot(3 * s), side(halves(s)[i])
+            third[s, i] = copies.send_to(ps.at[at, 1, :, cols], x_in.at[at, :, cols], mate)
+    for s in (1, 2, 0):
         back_to_mate(s)
 
-    o1, o2, o3, o4 = {}, {}, {}, {}
+    o3, o4 = {}, {}
     ps[7, 0] = with_mate(7).astype(BF16)
     for s in both:
         cols = side(halves(s)[0])
         o4[s] = send(ps.at[7, 0, :, cols], z4_in.at[slot(s) - 1], "z", 2 * s)
-    for s in both:
-        ps[slot(3 * s), 0] = with_mate(slot(3 * s)).astype(BF16)
     for i in range(2):
         for s in both:
-            cols = side(halves(s)[i])
+            at, cols = slot(3 * s), side(halves(s)[i])
+            third[s, i].wait_recv()
+            ps[at, 0, :, cols] = (ps[at, 0, :, cols].astype(F32) + x_in[at, :, cols].astype(F32)).astype(BF16)
             o3[s, i] = send(ps.at[slot(3 * s), 0, :, cols], z3_in.at[slot(s) - 1, :, cols], "z", s)
     for s in both:
         ps[slot(s), 0] = with_mate(slot(s)).astype(BF16)
-        o1[s] = send(ps.at[slot(s), 0], z_in.at[slot(s) - 1], "z", s)
+        spread_out(ps.at[slot(s), 0], slot(s) - 1, s)
+    ps[0, 0] = with_mate(0).astype(BF16)
+    spread_out(ps.at[0, 0], 4)
     relayed = {s: with_mate(slot(2 * s)) for s in both}
     for i in range(2):
         for s in both:
@@ -363,27 +395,14 @@
             if i == 0:
                 total = total + z4_in[slot(s) - 1].astype(F32)
             ps[there, 0, :, cols] = total.astype(BF16)
-            o2[s, i] = send(ps.at[there, 0, :, cols], z_in.at[slot(s) + 1, :, cols], "z", 2 * s)
-    down_sum = with_mate(0) + mid[...].astype(F32)
-    for s in both:
-        o1[s].wait_recv()
-        down_sum = down_sum + z_in[slot(s) - 1].astype(F32)
-    for s in both:
-        for i in range(2):
-            o2[s, i].wait_recv()
-        down_sum = down_sum + z_in[slot(s) + 1].astype(F32)
-    fin[...] = down_sum.astype(BF16)
-
-    def features(index):
-        return pl.ds(pl.multiple_of(index * width, width), width)
-
-    back = []
-    for peer in peers:
-        other = 2 * peer["y"] + peer["c"]
-        back.append(copies.send_to(fin.at[:, features(other)], out_ref.at[tp], peer))
-    out_ref[tp] = fin[:, features(tp)]
-    for copy in back:
+    for s in both:
+        spread_out(ps.at[slot(2 * s), 0], slot(s) + 1, 2 * s)
+    for copy in spread:
         copy.wait_recv()
+    total = 0.0
+    for place in range(6):
+        total = total + gathered[place].astype(F32)
+    out_ref[...] = total.astype(BF16)
     copies.finish()
 
 
@@ -442,7 +461,7 @@
     turn = np.concatenate([np.cos(angles), np.sin(angles)]).astype(np.float32)[:, None]
     vmem = pl.BlockSpec(memory_space=pltpu.VMEM)
     hbm = pl.BlockSpec(memory_space=pltpu.HBM)
-    copies = 80
+    copies = 128
     out, new_states = pl.pallas_call(
         layer_kernel,
         out_shape=(
@@ -476,11 +495,10 @@
             pltpu.VMEM((3, 16, D), BF16),
             pltpu.VMEM((3, 16, D), BF16),
             pltpu.VMEM((16, D), BF16),
-            pltpu.VMEM((16, D), BF16),
             pltpu.VMEM((8, 16, D), BF16),
             pltpu.VMEM((2, 16, D), BF16),
             pltpu.VMEM((2, 16, D // 2), BF16),
-            pltpu.VMEM((4, 16, D), BF16),
+            pltpu.VMEM((6, 8, 16, tokens.shape[1]), BF16),
             pltpu.SemaphoreType.DMA((12,)),
             pltpu.SemaphoreType.DMA((heads * size // 16,)),
             pltpu.SemaphoreType.DMA((copies,)),

time: 63.6 us -> 57.3 us (0.901)
  Pallas kernels: 62.9 us -> 56.5 us
    pallas_call x1, Pallas kernels: 60.8 us -> 54.4 us  [local(): pl.pallas_call(layer_kernel, out_shape=(pltpu.VMEM((8, 16, tokens.shape[1...]
where the time goes in v3:
time: 57.3 us; the launch traced here: 57.2 us
  Pallas kernels  56.5 us (99%)
  between operations  0.64 us (1%)
    pallas_call x1, Pallas kernels, local(): pl.pallas_call(layer_kernel, out_shape=(pltpu.VMEM((8, 16, tokens.shape[1...  54.4 us
    pallas_call x1, Pallas kernels, write_out(): pl.pallas_call(write_kernel, out_shape=(pltpu.HBM(out.shape, out.dtype),...  2.1 us

profile of v3, /device:TPU:1, one launch (start us, length us, event | category | flops | bytes accessed | tf_op | source)
XLA Modules:
  0.0 57.2 jit_solution(8971192562377473825)
XLA Ops:
  0.6 54.4 %layer.1 = (bf16[8,16,256]{2,1,0:T(8,128)(2,1)S(1)}, f32[2,64,64,128]{3,2,1,0:T(8,128)S(1)}) custom-call(bf16[128,256]{1,0:T(8,128)(2,1)} %tok_hbm.1, f32[2,64,64,128]{3,2,1,0:T(8,128)} %bitcast.6, bf16[16,128]{1,0:T(8,128)(2,1)} %bitcast.7, bf16[2048,128]{1,0:T(8,128)(2,1)} %wq_hbm.1, bf16[2048,128]{1,0:T(8,128)(2,1)} %wk_hbm.1, bf16[2048,128]{1,0:T(8,128)(2,1)} %wv_hbm.1, ...), custom_call_target="tpu_custom_call" | custom-call | tf_op jit(solution)/shard_map/layer/pallas_call | solution.py:465
  55.1 2.1 %write_out.1 = (bf16[8,16,256]{2,1,0:T(8,128)(2,1)}, f32[2,64,64,128]{3,2,1,0:T(8,128)}) custom-call(bf16[8,16,256]{2,1,0:T(8,128)(2,1)S(1)} %get-tuple-element.6.out_vmem, f32[2,64,64,128]{3,2,1,0:T(8,128)S(1)} %get-tuple-element.7.new_vmem), custom_call_target="tpu_custom_call" | custom-call | tf_op jit(solution)/shard_map/write_out/pallas_call | solution.py:426

commit v4 on v3

--- a/solution.py
+++ b/solution.py
@@ -92,10 +92,15 @@
     w_ref,
     wo_ref,
     states,
-    normed,
+    projected,
+    gain_rows,
     q_t,
     k_t,
+    v_t,
     gated_t,
+    gated_rows,
+    gated_in,
+    wo_pair,
     part,
     up_ref,
     down_ref,
@@ -104,8 +109,6 @@
     xs,
     ps,
     scaled,
-    pair_in,
-    y_sum,
     y_in,
     mid,
     x_in,
@@ -166,6 +169,8 @@
     for i in range(2):
         rows = pl.ds(pl.multiple_of((2 * c + i) * deep, deep), deep)
         weights.append((up_far.at[rows], send(up_ref.at[rows], up_far.at[rows], "x", 2)))
+    load_out.wait()
+    pair_out = send(wo_ref, wo_pair, "c", 1)
     handed = []
 
     def hand_over(i):
@@ -173,32 +178,40 @@
         copy.wait_recv()
         handed.append(send(there, there, "c", 1))
 
+    width = blocks.shape[2]
+    lanes = 128
+    for copy in load_small + load_w:
+        copy.wait()
+    gain_rows[...] = mix_gain_ref[...].astype(F32)
+
+    def project(index, squares):
+        block = blocks[index].astype(F32)
+        gains = [gain_rows[pl.ds(index * (width // lanes) + i, 1)] for i in range(width // lanes)]
+        scaled_block = (block * jnp.concatenate(gains, axis=1)).astype(BF16)
+        rows = pl.ds(pl.multiple_of(index * width, width), width)
+        product = jnp.dot(scaled_block, w_ref[rows], preferred_element_type=F32)
+        if squares is None:
+            projected[...] = product
+            return jnp.sum(block * block, axis=1, keepdims=True)
+        projected[...] += product
+        return squares + jnp.sum(block * block, axis=1, keepdims=True)
+
+    def block_of(step, core):
+        return 2 * lax.rem(y + (4 - step), 4) + core
+
+    total = project(tp, None)
     for step in (1, -1, 2):
         near[step].wait_recv()
-        arrived = blocks.at[2 * lax.rem(y + (4 - step), 4) + c]
+        arrived = blocks.at[block_of(step, c)]
         across.append(send(arrived, arrived, "c", 1))
-    for copy in across:
-        copy.wait_recv()
-
-    for copy in load_small:
-        copy.wait()
-    width = blocks.shape[2]
-    lanes = 128
-    mix_gain = mix_gain_ref[...].astype(F32)
-    total = 0.0
-    for i in range(8):
-        block = blocks[i].astype(F32)
-        total = total + jnp.sum(block * block, axis=1, keepdims=True)
+    for step in (1, -1, 2):
+        total = project(block_of(step, c), total)
+    for i, step in enumerate((0, 1, -1, 2)):
+        across[i].wait_recv()
+        total = project(block_of(step, 1 - c), total)
     inverse_rms = lax.rsqrt(total / D + EPSILON)
-    for i in range(D // lanes):
-        off = i * lanes % width
-        block = blocks[i * lanes // width, :, off : off + lanes].astype(F32)
-        normed[:, i * lanes : (i + 1) * lanes] = (block * inverse_rms * mix_gain[i : i + 1]).astype(BF16)
-    for copy in load_w:
-        copy.wait()
-    projected = jnp.dot(normed[...], w_ref[...], preferred_element_type=F32)
-
-    turned = [projected[:, 128 * i : 128 * (i + 1)].T for i in range(4)]
+
+    turned = [(projected[:, 128 * i : 128 * (i + 1)] * inverse_rms).T for i in range(4)]
     cosine, sines = turn_ref[0 : size // 2], turn_ref[size // 2 : size]
     for source, target, scale in ((turned[0], q_t, size ** (-0.5)), (turned[1], k_t, 1.0)):
         for h in range(heads):
@@ -206,61 +219,61 @@
             second = source[h * size + size // 2 : (h + 1) * size]
             target[h * size : h * size + size // 2] = (first * cosine - second * sines) * scale
             target[h * size + size // 2 : (h + 1) * size] = (first * sines + second * cosine) * scale
+    v_t[...] = turned[2]
+
+    def decay_of(h):
+        head = jnp.full((1, lanes), heads * tp + h).astype(F32)
+        return 1.0 - jnp.exp2(-1.0 - 11.0 * head / (HEADS - 1))
+
     for h in range(heads):
-        head = jnp.full((1, lanes), heads * tp + h).astype(F32)
-        decay = 1.0 - jnp.exp2(-1.0 - 11.0 * head / (HEADS - 1))
         rows = slice(h * size, (h + 1) * size)
         values = turned[2][rows]
-        output = jnp.zeros_like(values)
+        sums = jnp.zeros_like(values)
         for i, (span_head, ks) in enumerate(spans):
             if span_head != h:
                 continue
             load_states[i].wait()
 
-            def step(j, output):
-                for u in range(4):
-                    k = ks.start + 4 * j + u
-                    row = h * size + k
-                    new = decay * states[h, k] + k_t[pl.ds(row, 1)] * values
-                    new_ref[h, k] = new
-                    output = output + q_t[pl.ds(row, 1)] * new
-                return output
-
-            output = lax.fori_loop(0, chunk // 4, step, output)
+            def step(j, sums):
+                for u in range(8):
+                    k = ks.start + 8 * j + u
+                    sums = sums + q_t[pl.ds(h * size + k, 1)] * states[h, k]
+                return sums
+
+            sums = lax.fori_loop(0, chunk // 8, step, sums)
+        overlap = jnp.sum(q_t[rows] * k_t[rows], axis=0, keepdims=True)
+        output = decay_of(h) * sums + overlap * values
         center = output - jnp.mean(output, axis=0, keepdims=True)
         spread = jnp.mean(center * center, axis=0, keepdims=True)
         gate = turned[3][rows]
         gated_t[rows] = center * lax.rsqrt(spread + EPSILON) * (gate * jax.nn.sigmoid(gate))
     gated = (gated_t[...].T * head_gain_ref[...].astype(F32)).astype(BF16)
-    load_out.wait()
-    part[...] = jnp.dot(gated, wo_ref[...], preferred_element_type=F32).astype(BF16).reshape(8, 16, D)
-
-    def rows_for(offset, core):
-        return 2 * lax.rem(y + (offset + 4), 4) + core
+    gated_rows[...] = gated.reshape(4, 2, 16, heads * size)
+
+    traded = send(gated_rows.at[:, 1 - c], gated_in, "c", 1)
 
     def side(h):
         return slice(h * D // 2, (h + 1) * D // 2)
 
-    offsets = (2, 1, -1, 0)
-    across, near = {}, {}
+    offsets = (2, 1, -1)
+    near = {}
+    own_gated = gated_rows[:, c].reshape(64, heads * size)
+    firsts = [jnp.dot(own_gated, wo_ref[:, side(h)], preferred_element_type=F32) for h in range(2)]
+    pair_out.wait_recv()
+    traded.wait_recv()
+    other_gated = gated_in[...].reshape(64, heads * size)
     for h in range(2):
+        product = firsts[h] + jnp.dot(other_gated, wo_pair[:, side(h)], preferred_element_type=F32)
+        part[:, :, side(h)] = product.astype(BF16).reshape(4, 16, D // 2)
         for i, o in enumerate(offsets):
-            across[i, h] = send(part.at[rows_for(o, 1 - c), :, side(h)], pair_in.at[i, :, side(h)], "c", 1)
-
-    def pair_sum(i, h):
-        across[i, h].wait_recv()
-        return part[rows_for(offsets[i], c), :, side(h)].astype(F32) + pair_in[i, :, side(h)].astype(F32)
-
-    for h in range(2):
-        for i in range(3):
-            y_sum[i, :, side(h)] = pair_sum(i, h).astype(BF16)
-            near[i, h] = send(y_sum.at[i, :, side(h)], y_in.at[i, :, side(h)], "y", offsets[i])
+            there = part.at[lax.rem(y + (o + 4), 4), :, side(h)]
+            near[i, h] = send(there, y_in.at[i, :, side(h)], "y", o)
     mine = pl.ds(pl.multiple_of(16 * tp, 16), 16)
     own_rows = jnp.concatenate([blocks[i, mine] for i in range(8)], axis=1).astype(F32)
     z1, z2, z3, z4, xn = {}, {}, {}, {}, {}
     both_halves = (0, 1)
     for h in both_halves:
-        attended = pair_sum(3, h)
+        attended = part[y, :, side(h)].astype(F32)
         for i in (1, 2, 0):
             near[i, h].wait_recv()
             attended = attended + y_in[i, :, side(h)].astype(F32)
@@ -270,6 +283,9 @@
         for s in both:
             z2[s, h] = send(xs.at[0, 0, :, side(h)], xs.at[slot(-2 * s), 0, :, side(h)], "z", 2 * s)
 
+    def half_to_mate(s, h):
+        xn[s, h] = copies.send_to(xs.at[s, 0, :, side(h)], xs.at[s, 1, :, side(h)], mate)
+
     def to_mate(s):
         xn[s] = copies.send_to(xs.at[s, 0], xs.at[s, 1], mate)
 
@@ -297,6 +313,17 @@
     along = {step: send(down_rows(0, c), down_rows(0, c), "y", step) for step in (2, 1, -1)}
     handed.append(send(down_rows(0, c), down_rows(0, c), "c", 1))
     hand_over(0)
+    for h in range(heads):
+        decay = decay_of(h)
+        values = v_t[h * size : (h + 1) * size]
+
+        def renew(j, carry):
+            for u in range(8):
+                k = 8 * j + u
+                new_ref[h, k] = decay * states[h, k] + k_t[pl.ds(h * size + k, 1)] * values
+            return carry
+
+        lax.fori_loop(0, size // 8, renew, 0)
     for h in both_halves:
         for s in both:
             z2[s, h].wait_recv()
@@ -304,8 +331,7 @@
             if h == halves(s)[0]:
                 z4[s] = send(xs.at[came, 0, :, side(h)], xs.at[7, 0, :, side(h)], "z", 2 * s)
             z3[s, h] = send(xs.at[came, 0, :, side(h)], xs.at[slot(-3 * s), 0, :, side(h)], "z", s)
-            if h == 1:
-                to_mate(came)
+            half_to_mate(came, h)
     hand_over(1)
     spread_out(mid, 5)
     for s in both:
@@ -318,9 +344,11 @@
         z4[s].wait_recv()
     to_mate(7)
     for s in both:
-        for i in range(2):
-            z3[s, i].wait_recv()
-        to_mate(slot(-3 * s))
+        z3[s, 0].wait_recv()
+        half_to_mate(slot(-3 * s), 0)
+    for s in both:
+        z3[s, 1].wait_recv()
+        half_to_mate(slot(-3 * s), 1)
     gain = channel_gain_ref[...].astype(F32)
 
     def mix(first, stop):
@@ -341,8 +369,8 @@
 
     for copy in handed:
         copy.wait_recv()
-    for s in range(5):
-        xn[s].wait_recv()
+    for key in (0, (3, 0), (4, 0), (3, 1), (4, 1), 1, 2):
+        xn[key].wait_recv()
     mix(0, 5)
 
     xo = {}
@@ -354,10 +382,10 @@
         xo[s].wait_recv()
         return ps[s, 0].astype(F32) + x_in[s].astype(F32)
 
-    for s in (3, 4):
+    for s in (3, 4, 1):
         back_to_mate(s)
-    for s in (7, 5, 6):
-        xn[s].wait_recv()
+    for key in (7, (5, 0), (6, 0), (5, 1), (6, 1)):
+        xn[key].wait_recv()
     mix(5, 8)
     back_to_mate(7)
     third = {}
@@ -365,7 +393,7 @@
         for s in both:
             at, cols = slot(3 * s), side(halves(s)[i])
             third[s, i] = copies.send_to(ps.at[at, 1, :, cols], x_in.at[at, :, cols], mate)
-    for s in (1, 2, 0):
+    for s in (2, 0):
         back_to_mate(s)
 
     o3, o4 = {}, {}
@@ -395,8 +423,8 @@
             if i == 0:
                 total = total + z4_in[slot(s) - 1].astype(F32)
             ps[there, 0, :, cols] = total.astype(BF16)
-    for s in both:
-        spread_out(ps.at[slot(2 * s), 0], slot(s) + 1, 2 * s)
+            if i == 1:
+                spread_out(ps.at[there, 0], slot(s) + 1, 2 * s)
     for copy in spread:
         copy.wait_recv()
     total = 0.0
@@ -479,11 +507,16 @@
             pltpu.VMEM((D, 4 * heads * size), BF16),
             pltpu.VMEM((heads * size, D), BF16),
             pltpu.VMEM((heads, size, size, rows), F32),
-            pltpu.VMEM((rows, D), BF16),
+            pltpu.VMEM((rows, 4 * heads * size), F32),
+            pltpu.VMEM((D // 128, 128), F32),
             pltpu.VMEM((heads * size, rows), F32),
             pltpu.VMEM((heads * size, rows), F32),
             pltpu.VMEM((heads * size, rows), F32),
-            pltpu.VMEM((8, 16, D), BF16),
+            pltpu.VMEM((heads * size, rows), F32),
+            pltpu.VMEM((4, 2, 16, heads * size), BF16),
+            pltpu.VMEM((4, 16, heads * size), BF16),
+            pltpu.VMEM((heads * size, D), BF16),
+            pltpu.VMEM((4, 16, D), BF16),
             pltpu.VMEM((D, hidden), BF16),
             pltpu.VMEM((hidden, D), BF16),
             pltpu.VMEM((D, hidden), BF16),
@@ -491,8 +524,6 @@
             pltpu.VMEM((8, 2, 16, D), BF16),
             pltpu.VMEM((8, 2, 16, D), BF16),
             pltpu.VMEM((160, D), BF16),
-            pltpu.VMEM((4, 16, D), BF16),
-            pltpu.VMEM((3, 16, D), BF16),
             pltpu.VMEM((3, 16, D), BF16),
             pltpu.VMEM((16, D), BF16),
             pltpu.VMEM((8, 16, D), BF16),

time: 57.3 us -> 55.6 us (0.970)
  Pallas kernels: 56.5 us -> 54.9 us
    pallas_call x1, Pallas kernels: 54.4 us -> 52.8 us  [local(): pl.pallas_call(layer_kernel, out_shape=(pltpu.VMEM((8, 16, tokens.shape[1...]
where the time goes in v4:
time: 55.6 us
  Pallas kernels  54.9 us (99%)
  between operations  0.64 us (1%)
    pallas_call x1, Pallas kernels, local(): pl.pallas_call(layer_kernel, out_shape=(pltpu.VMEM((8, 16, tokens.shape[1...  52.8 us
    pallas_call x1, Pallas kernels, write_out(): pl.pallas_call(write_kernel, out_shape=(pltpu.HBM(out.shape, out.dtype),...  2.1 us

profile of v4, /device:TPU:1, one launch (start us, length us, event | category | flops | bytes accessed | tf_op | source)
XLA Modules:
  0.0 55.6 jit_solution(6082970661502264842)
XLA Ops:
  0.6 52.8 %layer.1 = (bf16[8,16,256]{2,1,0:T(8,128)(2,1)S(1)}, f32[2,64,64,128]{3,2,1,0:T(8,128)S(1)}) custom-call(bf16[128,256]{1,0:T(8,128)(2,1)} %tok_hbm.1, f32[2,64,64,128]{3,2,1,0:T(8,128)} %bitcast.6, bf16[16,128]{1,0:T(8,128)(2,1)} %bitcast.7, bf16[2048,128]{1,0:T(8,128)(2,1)} %wq_hbm.1, bf16[2048,128]{1,0:T(8,128)(2,1)} %wk_hbm.1, bf16[2048,128]{1,0:T(8,128)(2,1)} %wv_hbm.1, ...), custom_call_target="tpu_custom_call" | custom-call | tf_op jit(solution)/shard_map/layer/pallas_call | solution.py:493
  53.5 2.1 %write_out.1 = (bf16[8,16,256]{2,1,0:T(8,128)(2,1)}, f32[2,64,64,128]{3,2,1,0:T(8,128)}) custom-call(bf16[8,16,256]{2,1,0:T(8,128)(2,1)S(1)} %get-tuple-element.6.out_vmem, f32[2,64,64,128]{3,2,1,0:T(8,128)S(1)} %get-tuple-element.7.new_vmem), custom_call_target="tpu_custom_call" | custom-call | tf_op jit(solution)/shard_map/write_out/pallas_call | solution.py:454

commit v5 on v4

--- a/solution.py
+++ b/solution.py
@@ -295,8 +295,8 @@
     everyone = [{"y": lax.rem(y + dy, 4), "c": lax.rem(c + dc, 2)} for dy in (2, 1, 3, 0) for dc in (1, 0)]
     spread = []
 
-    def spread_out(row_ref, place, step=0):
-        for peer in everyone if step else everyone[:-1]:
+    def spread_out(row_ref, place, step=0, among=None):
+        for peer in among or (everyone if step else everyone[:-1]):
             other = 2 * peer["y"] + peer["c"]
             device = dict(peer, **neighbour("z", step)) if step else peer
             spread.append(copies.send_to(row_ref.at[:, features(other)], gathered.at[place, tp], device))
@@ -388,43 +388,50 @@
         xn[key].wait_recv()
     mix(5, 8)
     back_to_mate(7)
+    turns = (2, 1, 3, 0)
+
+    def quarter(q):
+        return pl.ds(pl.multiple_of(lax.rem(y + turns[q], 4) * (D // 4), D // 4), D // 4)
+
     third = {}
+    for q in range(4):
+        for s in both:
+            at, cols = slot(3 * s), quarter(q)
+            third[s, q] = copies.send_to(ps.at[at, 1, :, cols], x_in.at[at, :, cols], mate)
+    for s in (2, 0):
+        back_to_mate(s)
+
+    o3, o4 = {}, {}
+    ps[7, 0] = with_mate(7).astype(BF16)
+    farthest = {1: (0, 1), -1: (2, 3)}
     for i in range(2):
         for s in both:
-            at, cols = slot(3 * s), side(halves(s)[i])
-            third[s, i] = copies.send_to(ps.at[at, 1, :, cols], x_in.at[at, :, cols], mate)
-    for s in (2, 0):
-        back_to_mate(s)
-
-    o3, o4 = {}, {}
-    ps[7, 0] = with_mate(7).astype(BF16)
-    for s in both:
-        cols = side(halves(s)[0])
-        o4[s] = send(ps.at[7, 0, :, cols], z4_in.at[slot(s) - 1], "z", 2 * s)
-    for i in range(2):
+            q = farthest[s][i]
+            o4[s, q] = send(ps.at[7, 0, :, quarter(q)], z4_in.at[slot(s) - 1, :, quarter(q)], "z", 2 * s)
+    for q in range(4):
         for s in both:
-            at, cols = slot(3 * s), side(halves(s)[i])
-            third[s, i].wait_recv()
+            at, cols = slot(3 * s), quarter(q)
+            third[s, q].wait_recv()
             ps[at, 0, :, cols] = (ps[at, 0, :, cols].astype(F32) + x_in[at, :, cols].astype(F32)).astype(BF16)
-            o3[s, i] = send(ps.at[slot(3 * s), 0, :, cols], z3_in.at[slot(s) - 1, :, cols], "z", s)
+            o3[s, q] = send(ps.at[at, 0, :, cols], z3_in.at[slot(s) - 1, :, cols], "z", s)
     for s in both:
         ps[slot(s), 0] = with_mate(slot(s)).astype(BF16)
         spread_out(ps.at[slot(s), 0], slot(s) - 1, s)
     ps[0, 0] = with_mate(0).astype(BF16)
     spread_out(ps.at[0, 0], 4)
-    relayed = {s: with_mate(slot(2 * s)) for s in both}
-    for i in range(2):
+    for s in both:
+        xo[slot(2 * s)].wait_recv()
+    for q in range(4):
         for s in both:
-            there, cols = slot(2 * s), side(halves(s)[i])
-            if i == 0:
-                o4[s].wait_recv()
-            o3[s, i].wait_recv()
-            total = relayed[s][:, cols] + z3_in[slot(s) - 1, :, cols].astype(F32)
-            if i == 0:
-                total = total + z4_in[slot(s) - 1].astype(F32)
+            there, cols = slot(2 * s), quarter(q)
+            total = ps[there, 0, :, cols].astype(F32) + x_in[there, :, cols].astype(F32)
+            if q in farthest[s]:
+                o4[s, q].wait_recv()
+                total = total + z4_in[slot(s) - 1, :, cols].astype(F32)
+            o3[s, q].wait_recv()
+            total = total + z3_in[slot(s) - 1, :, cols].astype(F32)
             ps[there, 0, :, cols] = total.astype(BF16)
-            if i == 1:
-                spread_out(ps.at[there, 0], slot(s) + 1, 2 * s)
+            spread_out(ps.at[there, 0], slot(s) + 1, 2 * s, everyone[2 * q : 2 * q + 2])
     for copy in spread:
         copy.wait_recv()
     total = 0.0
@@ -489,7 +496,7 @@
     turn = np.concatenate([np.cos(angles), np.sin(angles)]).astype(np.float32)[:, None]
     vmem = pl.BlockSpec(memory_space=pltpu.VMEM)
     hbm = pl.BlockSpec(memory_space=pltpu.HBM)
-    copies = 128
+    copies = 136
     out, new_states = pl.pallas_call(
         layer_kernel,
         out_shape=(
@@ -528,7 +535,7 @@
             pltpu.VMEM((16, D), BF16),
             pltpu.VMEM((8, 16, D), BF16),
             pltpu.VMEM((2, 16, D), BF16),
-            pltpu.VMEM((2, 16, D // 2), BF16),
+            pltpu.VMEM((2, 16, D), BF16),
             pltpu.VMEM((6, 8, 16, tokens.shape[1]), BF16),
             pltpu.SemaphoreType.DMA((12,)),
             pltpu.SemaphoreType.DMA((heads * size // 16,)),

time: 55.6 us -> 55.2 us (level)
  no operation moved by 1% of the time
where the time goes in v5:
time: 55.2 us; the launch traced here: 55.1 us
  Pallas kernels  54.5 us (99%)
  between operations  0.64 us (1%)
    pallas_call x1, Pallas kernels, local(): pl.pallas_call(layer_kernel, out_shape=(pltpu.VMEM((8, 16, tokens.shape[1...  52.4 us
    pallas_call x1, Pallas kernels, write_out(): pl.pallas_call(write_kernel, out_shape=(pltpu.HBM(out.shape, out.dtype),...  2.1 us

profile of v5, /device:TPU:1, one launch (start us, length us, event | category | flops | bytes accessed | tf_op | source)
XLA Modules:
  0.0 55.1 jit_solution(17837917908111318502)
XLA Ops:
  0.6 52.4 %layer.1 = (bf16[8,16,256]{2,1,0:T(8,128)(2,1)S(1)}, f32[2,64,64,128]{3,2,1,0:T(8,128)S(1)}) custom-call(bf16[128,256]{1,0:T(8,128)(2,1)} %tok_hbm.1, f32[2,64,64,128]{3,2,1,0:T(8,128)} %bitcast.6, bf16[16,128]{1,0:T(8,128)(2,1)} %bitcast.7, bf16[2048,128]{1,0:T(8,128)(2,1)} %wq_hbm.1, bf16[2048,128]{1,0:T(8,128)(2,1)} %wk_hbm.1, bf16[2048,128]{1,0:T(8,128)(2,1)} %wv_hbm.1, ...), custom_call_target="tpu_custom_call" | custom-call | tf_op jit(solution)/shard_map/layer/pallas_call | solution.py:500
  53.0 2.1 %write_out.1 = (bf16[8,16,256]{2,1,0:T(8,128)(2,1)}, f32[2,64,64,128]{3,2,1,0:T(8,128)}) custom-call(bf16[8,16,256]{2,1,0:T(8,128)(2,1)S(1)} %get-tuple-element.6.out_vmem, f32[2,64,64,128]{3,2,1,0:T(8,128)S(1)} %get-tuple-element.7.new_vmem), custom_call_target="tpu_custom_call" | custom-call | tf_op jit(solution)/shard_map/write_out/pallas_call | solution.py:461

commit v6 on v5

--- a/solution.py
+++ b/solution.py
@@ -152,7 +152,7 @@
     send = copies.send
 
     own = blocks.at[tp]
-    near = {step: send(own, own, "y", step) for step in (2, 1, -1)}
+    near = {step: send(own, own, "y", step) for step in (1, -1, 2)}
     across = [send(own, own, "c", 1)]
 
     load_up.wait()
@@ -282,6 +282,7 @@
         mid[:, side(h)] = middle
         for s in both:
             z2[s, h] = send(xs.at[0, 0, :, side(h)], xs.at[slot(-2 * s), 0, :, side(h)], "z", 2 * s)
+        xn[0, h] = copies.send_to(xs.at[0, 0, :, side(h)], xs.at[0, 1, :, side(h)], mate)
 
     def half_to_mate(s, h):
         xn[s, h] = copies.send_to(xs.at[s, 0, :, side(h)], xs.at[s, 1, :, side(h)], mate)
@@ -308,7 +309,6 @@
 
     for s in both:
         z1[s] = send(xs.at[0, 0], xs.at[slot(-s), 0], "z", s)
-    to_mate(0)
     first_down.wait_recv()
     along = {step: send(down_rows(0, c), down_rows(0, c), "y", step) for step in (2, 1, -1)}
     handed.append(send(down_rows(0, c), down_rows(0, c), "c", 1))
@@ -369,7 +369,7 @@
 
     for copy in handed:
         copy.wait_recv()
-    for key in (0, (3, 0), (4, 0), (3, 1), (4, 1), 1, 2):
+    for key in ((0, 0), (0, 1), (3, 0), (4, 0), (3, 1), (4, 1), 1, 2):
         xn[key].wait_recv()
     mix(0, 5)
 

time: 55.2 us -> 55.2 us (level)
  no operation moved by 1% of the time
where the time goes in v6:
time: 55.2 us; the launch traced here: 55.1 us
  Pallas kernels  54.5 us (99%)
  between operations  0.64 us (1%)
    pallas_call x1, Pallas kernels, local(): pl.pallas_call(layer_kernel, out_shape=(pltpu.VMEM((8, 16, tokens.shape[1...  52.4 us
    pallas_call x1, Pallas kernels, write_out(): pl.pallas_call(write_kernel, out_shape=(pltpu.HBM(out.shape, out.dtype),...  2.1 us

profile of v6, /device:TPU:1, one launch (start us, length us, event | category | flops | bytes accessed | tf_op | source)
XLA Modules:
  0.0 55.1 jit_solution(10871389073269175422)
XLA Ops:
  0.6 52.4 %layer.1 = (bf16[8,16,256]{2,1,0:T(8,128)(2,1)S(1)}, f32[2,64,64,128]{3,2,1,0:T(8,128)S(1)}) custom-call(bf16[128,256]{1,0:T(8,128)(2,1)} %tok_hbm.1, f32[2,64,64,128]{3,2,1,0:T(8,128)} %bitcast.6, bf16[16,128]{1,0:T(8,128)(2,1)} %bitcast.7, bf16[2048,128]{1,0:T(8,128)(2,1)} %wq_hbm.1, bf16[2048,128]{1,0:T(8,128)(2,1)} %wk_hbm.1, bf16[2048,128]{1,0:T(8,128)(2,1)} %wv_hbm.1, ...), custom_call_target="tpu_custom_call" | custom-call | tf_op jit(solution)/shard_map/layer/pallas_call | solution.py:500
  53.0 2.1 %write_out.1 = (bf16[8,16,256]{2,1,0:T(8,128)(2,1)}, f32[2,64,64,128]{3,2,1,0:T(8,128)}) custom-call(bf16[8,16,256]{2,1,0:T(8,128)(2,1)S(1)} %get-tuple-element.6.out_vmem, f32[2,64,64,128]{3,2,1,0:T(8,128)S(1)} %get-tuple-element.7.new_vmem), custom_call_target="tpu_custom_call" | custom-call | tf_op jit(solution)/shard_map/write_out/pallas_call | solution.py:461
